TPU v7x, 32 devices: a whole 2x2x4 slice. The times are simulated.
32 devices in a mesh: sp: 8 (over z, y), dp: 4 (over x, core).
Axes of the slice: x: 2, y: 2, z: 4, core: 2. Of those that a mesh axis runs over, the one named last changes fastest.
Arguments:
- residual_input: bfloat16 [4, 1024, 2048], P('dp', 'sp'), may hold values from -6 to 6
- queries: bfloat16 [4, 1024, 512], P('dp', 'sp'), may hold values from -6 to 6
- keys: bfloat16 [4, 1024, 512], P('dp', 'sp'), may hold values from -6 to 6
- values: bfloat16 [4, 1024, 1024], P('dp', 'sp'), may hold values from -6 to 6
- gate_logits: bfloat16 [4, 1024, 32], P('dp', 'sp'), may hold values from -6 to 6
- retention_offset: float32 [8, 2], P('sp'), may hold values from 3 to 12
- log_forget_extra: float32 [4, 8, 1024], P('dp', 'sp'), may hold values from -2.76 to 0
- lane_amplifier: float32 [1024], P('sp'), may hold values from 0.1 to 1.9
- output_gate_logits: bfloat16 [4, 1024, 1024], P('dp', 'sp'), may hold values from -6 to 6
- output_projection: bfloat16 [1024, 2048], P(None, 'dp'), may hold values from -0.1875 to 0.1875
- cell_norm_gain: float32 [2048], replicated, may hold values from 0.1 to 1.9
- expert_norm_gain: float32 [2048], replicated, may hold values from 0.1 to 1.9
- expert_index: int32 [4, 1024, 2], P('dp', 'sp'), may hold values from 0 to 31, all different within a row; in each aligned block of 128 rows (0 to 127, 128 to 255, ..., all dimensions but the last counted through in order) at most 16 rows name the same one
- group_mixing_weight: float32 [4, 1024, 4], P('dp', 'sp'), may hold values from 0.05 to 1
- within_group_weight: float32 [4, 1024, 2], P('dp', 'sp'), may hold values from 0.1 to 1
- gate_weight: bfloat16 [32, 2048, 1024], P(('sp', 'dp')), may hold values from -0.125 to 0.125
- up_weight: bfloat16 [32, 2048, 1024], P(('sp', 'dp')), may hold values from -0.125 to 0.125
- down_weight: bfloat16 [32, 1024, 2048], P(('sp', 'dp')), may hold values from -0.75 to 0.75
Outputs:
- stream_out: bfloat16 [4, 1024, 2048], P('dp', 'sp')
Inputs may be any that keep to these rules, and one draw needn't show every extreme that they name: `expert_index`: A token's two experts differ; among the 128 tokens of one device no expert is named more than 16 times, a bound that some block reaches.
All inputs are finite; a program needn't handle non-finite values.
Results may differ from a plain program's by a relative error of at most 0.0095.
Values may be sent and summed in bfloat16 or wider, within the bound.
A program may use at most 128 MiB of HBM per device.

v0:
```python
from functools import partial

import jax
import jax.numpy as jnp
from jax import lax
from jax.experimental import pallas as pl
from jax.experimental.pallas import tpu as pltpu
from jax.sharding import PartitionSpec as P

EPS = 1e-06
MESH = pl.DeviceIdType.MESH
GATE_ROWS = 16
CHUNKS = 4
FF_TILE = 256
PIECES = 4


def log_sigmoid(x):
    return jnp.minimum(x, 0.0) - jnp.log1p(jnp.exp(-jnp.abs(x)))


def layer_kernel(*refs, n, dpn, inputs):
    hbm, (out_ref,), rest = refs[:inputs], refs[inputs : inputs + 1], refs[inputs + 1 :]
    local, rest = rest[:inputs], rest[inputs:]
    (
        q_ref, k_ref, v_ref, g_ref, offset_ref, extra_ref, amp_ref, logits_ref, w_ref,
        res_ref, cell_gain_ref, expert_gain_ref, index_ref, group_ref, within_ref,
        gate_ref, up_ref, down_ref,
    ) = local
    (
        send, recv, gates_t, cols, mixed, mrecv, wfull, proj,
        moe, table_t, table_0, table_1, outgoing, incoming, xs, hs, produced, returned,
        in_sem, send_sem, recv_sem, msend_sem, mrecv_sem, wx_send, wx_recv, wc_send, wc_recv,
        wl_sem, out_send, out_recv, back_send, back_recv,
    ) = rest
    loads = [pltpu.make_async_copy(hbm[i], local[i], in_sem.at[i]) for i in range(inputs)]
    for load in loads:
        load.start()
    tok = q_ref.shape[1]
    dk = q_ref.shape[2] // n
    dv = v_ref.shape[2] // n
    length = n * tok
    wcol = w_ref.shape[1]
    me = lax.axis_index("sp")
    my_dp = lax.axis_index("dp")
    my_x, my_core = my_dp // 2, my_dp % 2
    chips = dpn // 2

    barrier = pltpu.get_barrier_semaphore()

    devices = n * dpn
    mine = me * dpn + my_dp
    cap = 4 * tok // devices
    per = devices // CHUNKS
    my_chunk, my_place = mine // per, mine % per

    def greet(o, _):
        other = (mine + o) % devices
        pl.semaphore_signal(
            barrier,
            inc=1,
            device_id={"sp": other // dpn, "dp": other % dpn},
            device_id_type=MESH,
        )
        return 0

    lax.fori_loop(1, devices, greet, 0)
    for load in loads[:4]:
        load.wait()

    for h in range(n):
        send[h, 0:tok, 0:dk] = k_ref[0, :, h * dk : (h + 1) * dk]
        send[h, 0:tok, dk : 2 * dk] = q_ref[0, :, h * dk : (h + 1) * dk]
        send[h, 0:tok, 2 * dk : 2 * dk + dv] = v_ref[0, :, h * dv : (h + 1) * dv]
    g = g_ref[0].astype(jnp.float32)
    g = jnp.concatenate([g, jnp.zeros((tok, 128 - g.shape[1]), jnp.float32)], axis=1)
    gates_t[...] = g.T
    for h in range(n):
        send[h, tok : tok + GATE_ROWS, 0:tok] = gates_t[4 * h : 4 * h + GATE_ROWS, :].astype(
            jnp.bfloat16
        )
        send[h, tok : tok + GATE_ROWS, tok:] = jnp.zeros(
            (GATE_ROWS, send.shape[2] - tok), jnp.bfloat16
        )

    pl.semaphore_wait(barrier, devices - 1)

    def qkv_copy(o):
        return pltpu.make_async_remote_copy(
            src_ref=send.at[(me + o) % n],
            dst_ref=recv.at[me],
            send_sem=send_sem.at[o],
            recv_sem=recv_sem.at[o],
            device_id={"sp": (me + o) % n, "dp": my_dp},
            device_id_type=MESH,
        )

    def qkv_arrival(o):
        return pltpu.make_async_remote_copy(
            src_ref=send.at[(me + o) % n],
            dst_ref=recv.at[(me + n - o) % n],
            send_sem=send_sem.at[o],
            recv_sem=recv_sem.at[o],
            device_id={"sp": (me + o) % n, "dp": my_dp},
            device_id_type=MESH,
        )

    piece = w_ref.shape[0] // PIECES

    def wx_copy(o, p, slot):
        return pltpu.make_async_remote_copy(
            src_ref=w_ref.at[pl.ds(p * piece, piece)],
            dst_ref=wfull.at[slot, pl.ds(p * piece, piece)],
            send_sem=wx_send.at[o, p],
            recv_sem=wx_recv.at[o, p],
            device_id={"sp": me, "dp": ((my_x + o) % chips) * 2 + my_core},
            device_id_type=MESH,
        )

    def wc_copy(o, p, src, slot):
        return pltpu.make_async_remote_copy(
            src_ref=src.at[pl.ds(p * piece, piece)],
            dst_ref=wfull.at[slot, pl.ds(p * piece, piece)],
            send_sem=wc_send.at[o, p],
            recv_sem=wc_recv.at[o, p],
            device_id={"sp": me, "dp": my_x * 2 + 1 - my_core},
            device_id_type=MESH,
        )

    def from_chip(o):
        return ((my_x + chips - o) % chips) * 2 + my_core

    def pass_on(p):
        for o in range(1, chips):
            slot = from_chip(o)
            wx_copy(o, p, slot).wait_recv()
            wc_copy(o, p, wfull.at[slot], slot).start()

    for o in range(1, n):
        qkv_copy(o).start()
    loads[8].wait()
    for p in range(PIECES):
        for o in range(1, chips):
            wx_copy(o, p, my_dp).start()
        wc_copy(0, p, w_ref, my_dp).start()
    own_w = pltpu.make_async_copy(w_ref, wfull.at[my_dp], wl_sem)
    own_w.start()
    recv[me] = send[me]
    for i in (4, 5, 6, 7, 9, 10, 11, 12, 13, 14):
        loads[i].wait()

    rows_in = per * cap
    ids = index_ref[0].astype(jnp.float32)
    e_0, e_1 = ids[:, 0:1], ids[:, 1:2]
    wide = -(-devices // 128) * 128
    lane_e = lax.broadcasted_iota(jnp.int32, (tok, wide), 1).astype(jnp.float32)
    hit_0 = jnp.where(lane_e == e_0, 1.0, 0.0)
    hit_1 = jnp.where(lane_e == e_1, 1.0, 0.0)
    tri = jnp.where(
        lax.broadcasted_iota(jnp.int32, (tok, tok), 1)
        < lax.broadcasted_iota(jnp.int32, (tok, tok), 0),
        1.0,
        0.0,
    ).astype(jnp.bfloat16)
    rank_0 = jnp.dot(tri, hit_0.astype(jnp.bfloat16), preferred_element_type=jnp.float32)
    rank_1 = jnp.dot(tri, hit_1.astype(jnp.bfloat16), preferred_element_type=jnp.float32)
    rank_1 = rank_1 + jnp.sum(hit_0, axis=0, keepdims=True)
    place_0 = e_0 * cap + jnp.sum(hit_0 * rank_0, axis=1, keepdims=True)
    place_1 = e_1 * cap + jnp.sum(hit_1 * rank_1, axis=1, keepdims=True)
    lane_t = lax.broadcasted_iota(jnp.int32, (tok, tok), 1)
    turned = jnp.where(lane_t == 0, place_0, place_1).T
    row_0, row_1 = turned[0:1], turned[1:2]
    sub_r = lax.broadcasted_iota(jnp.int32, (rows_in, tok), 0).astype(jnp.float32)
    lane_r = lax.broadcasted_iota(jnp.int32, (tok, rows_in), 1).astype(jnp.float32)
    for c in range(CHUNKS):
        at = sub_r + c * rows_in
        table_t[c] = (jnp.where(at == row_0, 1.0, 0.0) + jnp.where(at == row_1, 1.0, 0.0)).astype(
            jnp.bfloat16
        )
        at = lane_r + c * rows_in
        table_0[c] = jnp.where(at == place_0, 1.0, 0.0).astype(jnp.bfloat16)
        table_1[c] = jnp.where(at == place_1, 1.0, 0.0).astype(jnp.bfloat16)
    groups = group_ref.shape[2]
    span = devices // groups
    route_0 = jnp.zeros((tok, 1), jnp.float32)
    route_1 = jnp.zeros((tok, 1), jnp.float32)
    for c in range(groups):
        weight_c = group_ref[0, :, c : c + 1]
        route_0 += jnp.where((e_0 >= c * span) & (e_0 < (c + 1) * span), weight_c, 0.0)
        route_1 += jnp.where((e_1 >= c * span) & (e_1 < (c + 1) * span), weight_c, 0.0)
    route_0 = route_0 * within_ref[0, :, 0:1]
    route_1 = route_1 * within_ref[0, :, 1:2]

    for o in range(1, n):
        qkv_arrival(o).wait_recv()

    gates = jnp.concatenate(
        [recv[d, tok : tok + GATE_ROWS, 0:tok].astype(jnp.float32) for d in range(n)], axis=1
    )
    extra = extra_ref[0]
    f = log_sigmoid(gates[1:2] + offset_ref[0:1, 0:1]) + extra
    b = log_sigmoid(gates[3:4] + offset_ref[0:1, 1:2]) + extra
    f = jnp.broadcast_to(f, (8, length))
    b = jnp.broadcast_to(b, (8, length))
    lane = lax.broadcasted_iota(jnp.int32, (8, length), 1)
    step = 1
    while step < length:
        f = f + jnp.where(lane >= step, pltpu.roll(f, step, 1), 0.0)
        b = b + jnp.where(lane < length - step, pltpu.roll(b, length - step, 1), 0.0)
        step *= 2
    row_i = gates[0:1]
    row_f = row_i - f[0:1]
    row_b = gates[2:3] - b[0:1]
    sub = lax.broadcasted_iota(jnp.int32, (128, length), 0)
    stacked = jnp.where(sub == 0, f[0:1], jnp.where(sub == 1, b[0:1], row_i))
    cols[...] = stacked.T

    scale = dk ** (-0.5)
    amp = amp_ref[...]

    def mixed_copy(o, slot):
        return pltpu.make_async_remote_copy(
            src_ref=mixed.at[(me + o) % n],
            dst_ref=mrecv.at[slot],
            send_sem=msend_sem.at[o],
            recv_sem=mrecv_sem.at[o],
            device_id={"sp": (me + o) % n, "dp": my_dp},
            device_id_type=MESH,
        )

    def segment(j, _):
        d = (me + 1 + j) % n
        start = pl.multiple_of(d * tok, tok)
        kq = recv[d, 0:tok, 0 : 2 * dk]
        qs = kq[:, dk:].astype(jnp.float32) * scale
        ks = kq[:, :dk].astype(jnp.float32)
        diag = jnp.sum(qs * ks, axis=1, keepdims=True)
        qs = jnp.concatenate([qs, jnp.zeros_like(qs)], axis=1).astype(jnp.bfloat16)
        kall = recv[:, 0:tok, 0 : 2 * dk].reshape(length, 2 * dk)
        vall = recv[:, 0:tok, 2 * dk : 2 * dk + dv].reshape(length, dv)
        scores = lax.dot_general(
            qs, kall, (((1,), (1,)), ((), ())), preferred_element_type=jnp.float32
        )
        col = cols[pl.ds(start, tok), :]
        col_f, col_b, col_i = col[:, 0:1], col[:, 1:2], col[:, 2:3]
        t_pos = start + lax.broadcasted_iota(jnp.int32, (tok, length), 0)
        s_pos = lax.broadcasted_iota(jnp.int32, (tok, length), 1)
        before = s_pos < t_pos
        weight = scores * jnp.exp(jnp.where(before, col_f + row_f, col_b + row_b))
        diag = diag * jnp.exp(col_i)
        z_f = jnp.sum(jnp.where(before, weight, 0.0), axis=1, keepdims=True) + diag
        z_b = jnp.sum(jnp.where(before, 0.0, weight), axis=1, keepdims=True)
        inv_f = 1.0 / jnp.maximum(jnp.abs(z_f), 1.0)
        inv_b = 1.0 / jnp.maximum(jnp.abs(z_b), 1.0)
        probs = (weight * jnp.where(before, inv_f, inv_b)).astype(jnp.bfloat16)
        total = jnp.dot(probs, vall, preferred_element_type=jnp.float32)
        total = total + (diag * inv_f) * recv[d, 0:tok, 2 * dk : 2 * dk + dv].astype(jnp.float32)
        total = total * lax.rsqrt(jnp.mean(total * total, axis=1, keepdims=True) + EPS) * amp
        mixed[d] = total.astype(jnp.bfloat16)

        @pl.when(j >= 1)
        def _():
            mixed_copy(j, me).start()

        @pl.when(j == n // 2)
        def _():
            pass_on(PIECES - 2)

        return 0

    for p in range(PIECES - 2):
        pass_on(p)
    lax.fori_loop(0, n, segment, 0)
    pass_on(PIECES - 1)
    mrecv[me] = mixed[me]
    sig = jax.nn.sigmoid(logits_ref[0].astype(jnp.float32))
    for o in range(1, n):
        mixed_copy(o, (me + n - o) % n).wait_recv()
    gated = jnp.concatenate([mrecv[h].astype(jnp.float32) for h in range(n)], axis=1) * sig
    gated = gated.astype(jnp.bfloat16)
    own_w.wait()
    partner = 1 - my_core
    for p in range(PIECES):
        wc_copy(0, p, w_ref, my_x * 2 + partner).wait_recv()
        for o in range(1, chips):
            slot = ((my_x + chips - o) % chips) * 2 + partner
            wc_copy(o, p, wfull.at[slot], slot).wait_recv()
    for j in range(dpn):
        proj[:, j * wcol : (j + 1) * wcol] = jnp.dot(
            gated, wfull[j], preferred_element_type=jnp.float32
        )
    p = proj[...]
    stream = (
        res_ref[0].astype(jnp.float32)
        + cell_gain_ref[...] * p * lax.rsqrt(jnp.mean(p * p, axis=1, keepdims=True) + EPS)
    ).astype(jnp.bfloat16)
    s = stream.astype(jnp.float32)
    proj[...] = s
    moe[...] = (
        expert_gain_ref[...] * s * lax.rsqrt(jnp.mean(s * s, axis=1, keepdims=True) + EPS)
    ).astype(jnp.bfloat16)

    width = moe.shape[1]

    def copy_of(src, dst, sems, tag, dev, slot_src, slot_dst):
        return pltpu.make_async_remote_copy(
            src_ref=src.at[slot_src],
            dst_ref=dst.at[slot_dst],
            send_sem=sems[0].at[tag],
            recv_sem=sems[1].at[tag],
            device_id={"sp": dev // dpn, "dp": dev % dpn},
            device_id_type=MESH,
        )

    def ahead(z, i):
        return (my_chunk + z) % CHUNKS * per + (my_place + i) % per

    def behind(z, i):
        return (my_chunk + CHUNKS - z) % CHUNKS * per + (my_place + per - i) % per

    out_sems, back_sems = (out_send, out_recv), (back_send, back_recv)

    def each(z, act):
        def one(i, _):
            @pl.when(z * per + i > 0)
            def _():
                act(i)

            return 0

        lax.fori_loop(0, per, one, 0)

    def dispatch(turn, _):
        z = (turn + 1) % CHUNKS
        c = (my_chunk + z) % CHUNKS
        block = jnp.dot(table_t[c], moe[...], preferred_element_type=jnp.float32)
        outgoing[pl.ds(c * per, per)] = block.astype(jnp.bfloat16).reshape(per, cap, width)

        def start(i):
            dev = ahead(z, i)
            copy_of(outgoing, incoming, out_sems, z * per + i, dev, dev, mine).start()

        each(z, start)
        return 0

    lax.fori_loop(0, CHUNKS, dispatch, 0)
    incoming[mine] = outgoing[mine]
    for i in (15, 16, 17):
        loads[i].wait()
    ff = hs.shape[1]

    def expert(turn, _):
        z = (turn + 1) % CHUNKS
        c = (my_chunk + CHUNKS - z) % CHUNKS

        def arrive(i):
            dev = behind(z, i)
            copy_of(outgoing, incoming, out_sems, z * per + i, dev, dev, dev).wait_recv()

        each(z, arrive)
        xs[...] = incoming[pl.ds(c * per, per)].reshape(rows_in, width)

        def up_tile(t, _):
            at = pl.ds(pl.multiple_of(t * FF_TILE, FF_TILE), FF_TILE)
            x = xs[...]
            a = jnp.dot(x, gate_ref[0, :, at], preferred_element_type=jnp.float32)
            u = jnp.dot(x, up_ref[0, :, at], preferred_element_type=jnp.float32)
            hs[:, at] = (jax.nn.silu(a) * u).astype(jnp.bfloat16)
            return 0

        lax.fori_loop(0, ff // FF_TILE, up_tile, 0)

        def down_tile(t, _):
            at = pl.ds(pl.multiple_of(t * FF_TILE, FF_TILE), FF_TILE)
            y = jnp.dot(hs[...], down_ref[0, :, at], preferred_element_type=jnp.float32)
            produced[pl.ds(c * per, per), :, at] = y.astype(jnp.bfloat16).reshape(
                per, cap, FF_TILE
            )
            return 0

        lax.fori_loop(0, width // FF_TILE, down_tile, 0)

        def start(i):
            dev = behind(z, i)
            copy_of(produced, returned, back_sems, z * per + i, dev, dev, mine).start()

        each(z, start)
        return 0

    lax.fori_loop(0, CHUNKS, expert, 0)
    returned[mine] = produced[mine]

    def combine(turn, _):
        z = (turn + 1) % CHUNKS
        c = (my_chunk + z) % CHUNKS

        def arrive(i):
            dev = ahead(z, i)
            copy_of(produced, returned, back_sems, z * per + i, dev, dev, dev).wait_recv()

        each(z, arrive)
        block = returned[pl.ds(c * per, per)].reshape(rows_in, width)
        proj[...] += route_0 * jnp.dot(
            table_0[c], block, preferred_element_type=jnp.float32
        ) + route_1 * jnp.dot(table_1[c], block, preferred_element_type=jnp.float32)
        return 0

    lax.fori_loop(0, CHUNKS, combine, 0)
    out_ref[0] = proj[...].astype(jnp.bfloat16)

    def drain(z, _):
        def left(i):
            dev = ahead(z, i)
            copy_of(outgoing, incoming, out_sems, z * per + i, dev, dev, mine).wait_send()
            dev = behind(z, i)
            copy_of(produced, returned, back_sems, z * per + i, dev, dev, mine).wait_send()

        each(z, left)
        return 0

    lax.fori_loop(0, CHUNKS, drain, 0)
    for o in range(1, n):
        qkv_copy(o).wait_send()
        mixed_copy(o, me).wait_send()
    for p in range(PIECES):
        for o in range(1, chips):
            wx_copy(o, p, my_dp).wait_send()
            slot = from_chip(o)
            wc_copy(o, p, wfull.at[slot], slot).wait_send()
        wc_copy(0, p, w_ref, my_dp).wait_send()


def on_device(
    residual_input,
    queries,
    keys,
    values,
    gate_logits,
    retention_offset,
    log_forget_extra,
    lane_amplifier,
    output_gate_logits,
    output_projection,
    cell_norm_gain,
    expert_norm_gain,
    expert_index,
    group_mixing_weight,
    within_group_weight,
    gate_weight,
    up_weight,
    down_weight,
):
    n, dpn = lax.axis_size("sp"), lax.axis_size("dp")
    tok, width = residual_input.shape[1:]
    dk, dv = queries.shape[2] // n, values.shape[2] // n
    length, devices, ff = n * tok, n * dpn, gate_weight.shape[2]
    cap, per = 4 * tok // devices, devices // CHUNKS
    rows_in = per * cap
    operands = (
        queries, keys, values, gate_logits, retention_offset, log_forget_extra,
        lane_amplifier.reshape(1, dv), output_gate_logits, output_projection,
        residual_input, cell_norm_gain.reshape(1, width), expert_norm_gain.reshape(1, width),
        expert_index, group_mixing_weight, within_group_weight,
        gate_weight, up_weight, down_weight,
    )
    dma = pltpu.SemaphoreType.DMA
    bf16, f32 = jnp.bfloat16, jnp.float32
    hbm = pl.BlockSpec(memory_space=pltpu.HBM)
    return pl.pallas_call(
        partial(layer_kernel, n=n, dpn=dpn, inputs=len(operands)),
        out_shape=jax.ShapeDtypeStruct((1, tok, width), bf16),
        in_specs=[hbm] * len(operands),
        out_specs=pl.BlockSpec(memory_space=pltpu.VMEM),
        scratch_shapes=[pltpu.VMEM(x.shape, x.dtype) for x in operands]
        + [
            pltpu.VMEM((n, tok + GATE_ROWS, 2 * dk + dv), bf16),
            pltpu.VMEM((n, tok + GATE_ROWS, 2 * dk + dv), bf16),
            pltpu.VMEM((128, tok), f32),
            pltpu.VMEM((length, 128), f32),
            pltpu.VMEM((n, tok, dv), bf16),
            pltpu.VMEM((n, tok, dv), bf16),
            pltpu.VMEM((dpn,) + output_projection.shape, bf16),
            pltpu.VMEM((tok, width), f32),
            pltpu.VMEM((tok, width), bf16),
            pltpu.VMEM((CHUNKS, rows_in, tok), bf16),
            pltpu.VMEM((CHUNKS, tok, rows_in), bf16),
            pltpu.VMEM((CHUNKS, tok, rows_in), bf16),
            pltpu.VMEM((devices, cap, width), bf16),
            pltpu.VMEM((devices, cap, width), bf16),
            pltpu.VMEM((rows_in, width), bf16),
            pltpu.VMEM((rows_in, ff), bf16),
            pltpu.VMEM((devices, cap, width), bf16),
            pltpu.VMEM((devices, cap, width), bf16),
            dma((len(operands),)),
            dma((n,)), dma((n,)), dma((n,)), dma((n,)),
            dma((dpn // 2, PIECES)), dma((dpn // 2, PIECES)),
            dma((dpn // 2, PIECES)), dma((dpn // 2, PIECES)),
            dma(()),
            dma((devices,)), dma((devices,)), dma((devices,)), dma((devices,)),
        ],
        compiler_params=pltpu.CompilerParams(
            collective_id=0, has_side_effects=True, vmem_limit_bytes=60 * 1024 * 1024
        ),
    )(*operands)


def solution(mesh):
    in_specs = (
        P("dp", "sp", None),
        P("dp", "sp", None),
        P("dp", "sp", None),
        P("dp", "sp", None),
        P("dp", "sp", None),
        P("sp", None),
        P("dp", "sp", None),
        P("sp"),
        P("dp", "sp", None),
        P(None, "dp"),
        P(),
        P(),
        P("dp", "sp", None),
        P("dp", "sp", None),
        P("dp", "sp", None),
        P(("sp", "dp"), None, None),
        P(("sp", "dp"), None, None),
        P(("sp", "dp"), None, None),
    )
    out_specs = P("dp", "sp", None)
    return jax.shard_map(
        on_device, mesh=mesh, in_specs=in_specs, out_specs=out_specs, check_vma=False
    )
```

profile of v0, /device:TPU:0, one launch (start us, length us, event | category | flops | bytes accessed | tf_op | source)
XLA Modules:
  0.0 146.4 jit_solution(17075006269301743969)
XLA Ops:
  0.0 1.4 copy.19.refs_3_
  1.4 1.4 copy.20.refs_12_
  2.8 1.4 copy.21.refs_13_
  4.2 1.4 copy.22.refs_14_
  5.6 138.9 %shard_map.172 = bf16[1,128,2048]{2,1,0:T(8,128)(2,1)} custom-call(bf16[1,128,512]{2,1,0:T(8,128)(2,1)} %refs_0_.1, bf16[1,128,512]{2,1,0:T(8,128)(2,1)} %refs_1_.1, bf16[1,128,1024]{2,1,0:T(8,128)(2,1)} %refs_2_.1, bf16[1,128,32]{2,1,0:T(8,128)(2,1)} %copy.19.refs_3_, f32[1,2]{1,0:T(1,128)} %refs_4_.1, f32[1,1,1024]{2,1,0:T(1,128)} %refs_5_.1, ...), custom_call_target="tpu_custom_call" | custom-call | tf_op jit(solution)/shard_map/pallas_call | solution.py:469
  144.6 1.9 %copy.24 = bf16[1,128,2048]{2,1,0:T(8,128)(2,1)} copy(bf16[1,128,2048]{2,1,0:T(8,128)(2,1)} %shard_map.172) | data formatting | bytes 1048576
where the time goes:
time: 147 us; the launch traced here: 146 us
  Pallas kernels  139 us (95%)
  local copies, waits for them, and re-layouts  7.5 us (5%)
    pallas_call x1, Pallas kernels, on_device(): pl.pallas_call(partial(layer_kernel, n=n, dpn=dpn, inputs=len(operands)),...  139 us
    unnamed x5, local copies, waits for them, and re-layouts  7.5 us

commit v1 on v0

--- a/solution.py
+++ b/solution.py
@@ -10,7 +10,7 @@
 EPS = 1e-06
 MESH = pl.DeviceIdType.MESH
 GATE_ROWS = 16
-CHUNKS = 4
+PARTS = 4
 FF_TILE = 256
 PIECES = 4
 
@@ -29,9 +29,11 @@
     ) = local
     (
         send, recv, gates_t, cols, mixed, mrecv, wfull, proj,
-        moe, table_t, table_0, table_1, outgoing, incoming, xs, hs, produced, returned,
+        meta, table_t, table_hi, table_lo, line, outgoing, incoming, hs, produced, returned,
+        partial_out, partial_in, total,
         in_sem, send_sem, recv_sem, msend_sem, mrecv_sem, wx_send, wx_recv, wc_send, wc_recv,
-        wl_sem, out_send, out_recv, back_send, back_recv,
+        wl_sem, meta_send, meta_recv, up_send, down_send, line_recv,
+        out_send, out_recv, back_send, back_recv, part_send, part_recv,
     ) = rest
     loads = [pltpu.make_async_copy(hbm[i], local[i], in_sem.at[i]) for i in range(inputs)]
     for load in loads:
@@ -49,22 +51,30 @@
     barrier = pltpu.get_barrier_semaphore()
 
     devices = n * dpn
-    mine = me * dpn + my_dp
     cap = 4 * tok // devices
-    per = devices // CHUNKS
-    my_chunk, my_place = mine // per, mine % per
-
-    def greet(o, _):
-        other = (mine + o) % devices
+    ny = chips if n % chips == 0 else 1
+    nz = n // ny
+    plane = ny * dpn
+    my_z, my_y = me // ny, me % ny
+    my_q = my_y * dpn + my_dp
+
+    def device(z, q):
+        return {"sp": z * ny + q // dpn, "dp": q % dpn}
+
+    def greet_sp(o, _):
         pl.semaphore_signal(
-            barrier,
-            inc=1,
-            device_id={"sp": other // dpn, "dp": other % dpn},
-            device_id_type=MESH,
+            barrier, inc=1, device_id={"sp": (me + o) % n, "dp": my_dp}, device_id_type=MESH
         )
         return 0
 
-    lax.fori_loop(1, devices, greet, 0)
+    def greet_plane(o, _):
+        pl.semaphore_signal(
+            barrier, inc=1, device_id=device(my_z, (my_q + o) % plane), device_id_type=MESH
+        )
+        return 0
+
+    lax.fori_loop(1, n, greet_sp, 0)
+    lax.fori_loop(1, plane, greet_plane, 0)
     for load in loads[:4]:
         load.wait()
 
@@ -83,7 +93,7 @@
             (GATE_ROWS, send.shape[2] - tok), jnp.bfloat16
         )
 
-    pl.semaphore_wait(barrier, devices - 1)
+    pl.semaphore_wait(barrier, n - 1 + plane - 1)
 
     def qkv_copy(o):
         return pltpu.make_async_remote_copy(
@@ -149,7 +159,7 @@
     for i in (4, 5, 6, 7, 9, 10, 11, 12, 13, 14):
         loads[i].wait()
 
-    rows_in = per * cap
+    rows_in = plane * cap
     ids = index_ref[0].astype(jnp.float32)
     e_0, e_1 = ids[:, 0:1], ids[:, 1:2]
     wide = -(-devices // 128) * 128
@@ -167,19 +177,6 @@
     rank_1 = rank_1 + jnp.sum(hit_0, axis=0, keepdims=True)
     place_0 = e_0 * cap + jnp.sum(hit_0 * rank_0, axis=1, keepdims=True)
     place_1 = e_1 * cap + jnp.sum(hit_1 * rank_1, axis=1, keepdims=True)
-    lane_t = lax.broadcasted_iota(jnp.int32, (tok, tok), 1)
-    turned = jnp.where(lane_t == 0, place_0, place_1).T
-    row_0, row_1 = turned[0:1], turned[1:2]
-    sub_r = lax.broadcasted_iota(jnp.int32, (rows_in, tok), 0).astype(jnp.float32)
-    lane_r = lax.broadcasted_iota(jnp.int32, (tok, rows_in), 1).astype(jnp.float32)
-    for c in range(CHUNKS):
-        at = sub_r + c * rows_in
-        table_t[c] = (jnp.where(at == row_0, 1.0, 0.0) + jnp.where(at == row_1, 1.0, 0.0)).astype(
-            jnp.bfloat16
-        )
-        at = lane_r + c * rows_in
-        table_0[c] = jnp.where(at == place_0, 1.0, 0.0).astype(jnp.bfloat16)
-        table_1[c] = jnp.where(at == place_1, 1.0, 0.0).astype(jnp.bfloat16)
     groups = group_ref.shape[2]
     span = devices // groups
     route_0 = jnp.zeros((tok, 1), jnp.float32)
@@ -190,6 +187,24 @@
         route_1 += jnp.where((e_1 >= c * span) & (e_1 < (c + 1) * span), weight_c, 0.0)
     route_0 = route_0 * within_ref[0, :, 0:1]
     route_1 = route_1 * within_ref[0, :, 1:2]
+    lane_t = lax.broadcasted_iota(jnp.int32, (tok, 128), 1)
+    packed = jnp.where(
+        lane_t == 0, place_0, jnp.where(lane_t == 1, place_1, jnp.where(lane_t == 2, route_0, route_1))
+    )
+    meta[my_z] = packed.T[0:8]
+
+    def meta_copy(z, slot):
+        return pltpu.make_async_remote_copy(
+            src_ref=meta.at[my_z],
+            dst_ref=meta.at[slot],
+            send_sem=meta_send.at[z],
+            recv_sem=meta_recv.at[slot],
+            device_id=device(z, my_q),
+            device_id_type=MESH,
+        )
+
+    for o in range(1, nz):
+        meta_copy((my_z + o) % nz, my_z).start()
 
     for o in range(1, n):
         qkv_arrival(o).wait_recv()
@@ -273,6 +288,26 @@
     lax.fori_loop(0, n, segment, 0)
     pass_on(PIECES - 1)
     mrecv[me] = mixed[me]
+    sub_r = lax.broadcasted_iota(jnp.int32, (rows_in, tok), 0).astype(jnp.float32)
+    at = sub_r + (my_z * rows_in).astype(jnp.float32)
+
+    def tables(o, _):
+        z = (my_z + o) % nz
+
+        @pl.when(o > 0)
+        def _():
+            meta_copy(z, z).wait_recv()
+
+        rows = meta[z]
+        hit_0, hit_1 = at == rows[0:1], at == rows[1:2]
+        table_t[z] = (jnp.where(hit_0, 1.0, 0.0) + jnp.where(hit_1, 1.0, 0.0)).astype(jnp.bfloat16)
+        weighted = (jnp.where(hit_0, rows[2:3], 0.0) + jnp.where(hit_1, rows[3:4], 0.0)).T
+        high = weighted.astype(jnp.bfloat16)
+        table_hi[z] = high
+        table_lo[z] = (weighted - high.astype(jnp.float32)).astype(jnp.bfloat16)
+        return 0
+
+    lax.fori_loop(0, nz, tables, 0)
     sig = jax.nn.sigmoid(logits_ref[0].astype(jnp.float32))
     for o in range(1, n):
         mixed_copy(o, (me + n - o) % n).wait_recv()
@@ -295,74 +330,116 @@
         + cell_gain_ref[...] * p * lax.rsqrt(jnp.mean(p * p, axis=1, keepdims=True) + EPS)
     ).astype(jnp.bfloat16)
     s = stream.astype(jnp.float32)
-    proj[...] = s
-    moe[...] = (
+    width = s.shape[1]
+    part = width // PARTS
+    moe = (
         expert_gain_ref[...] * s * lax.rsqrt(jnp.mean(s * s, axis=1, keepdims=True) + EPS)
     ).astype(jnp.bfloat16)
 
-    width = moe.shape[1]
-
-    def copy_of(src, dst, sems, tag, dev, slot_src, slot_dst):
-        return pltpu.make_async_remote_copy(
-            src_ref=src.at[slot_src],
-            dst_ref=dst.at[slot_dst],
-            send_sem=sems[0].at[tag],
-            recv_sem=sems[1].at[tag],
-            device_id={"sp": dev // dpn, "dp": dev % dpn},
-            device_id_type=MESH,
-        )
-
-    def ahead(z, i):
-        return (my_chunk + z) % CHUNKS * per + (my_place + i) % per
-
-    def behind(z, i):
-        return (my_chunk + CHUNKS - z) % CHUNKS * per + (my_place + per - i) % per
-
-    out_sems, back_sems = (out_send, out_recv), (back_send, back_recv)
-
-    def each(z, act):
-        def one(i, _):
-            @pl.when(z * per + i > 0)
-            def _():
-                act(i)
-
-            return 0
-
-        lax.fori_loop(0, per, one, 0)
-
-    def dispatch(turn, _):
-        z = (turn + 1) % CHUNKS
-        c = (my_chunk + z) % CHUNKS
-        block = jnp.dot(table_t[c], moe[...], preferred_element_type=jnp.float32)
-        outgoing[pl.ds(c * per, per)] = block.astype(jnp.bfloat16).reshape(per, cap, width)
-
-        def start(i):
-            dev = ahead(z, i)
-            copy_of(outgoing, incoming, out_sems, z * per + i, dev, dev, mine).start()
-
-        each(z, start)
-        return 0
-
-    lax.fori_loop(0, CHUNKS, dispatch, 0)
-    incoming[mine] = outgoing[mine]
+    def line_copy(z, p, to, sems):
+        return pltpu.make_async_remote_copy(
+            src_ref=line.at[z, p],
+            dst_ref=line.at[z, p],
+            send_sem=sems.at[z, p],
+            recv_sem=line_recv.at[z, p],
+            device_id=device(to, my_q),
+            device_id_type=MESH,
+        )
+
+    above, below = (my_z + 1) % nz, (my_z + nz - 1) % nz
+    has_above, has_below = my_z + 1 < nz, my_z > 0
+    edge = (my_z == 0) | (my_z == nz - 1)
+
+    def spread(z, p):
+        @pl.when((z <= my_z) & has_above)
+        def _():
+            line_copy(z, p, above, up_send).start()
+
+        @pl.when((z >= my_z) & has_below)
+        def _():
+            line_copy(z, p, below, down_send).start()
+
+    for p in range(PARTS):
+        line[my_z, p] = moe[:, p * part : (p + 1) * part]
+        spread(my_z, p)
+    for p in range(PARTS):
+        total[p] = s[:, p * part : (p + 1) * part]
     for i in (15, 16, 17):
         loads[i].wait()
     ff = hs.shape[1]
 
-    def expert(turn, _):
-        z = (turn + 1) % CHUNKS
-        c = (my_chunk + CHUNKS - z) % CHUNKS
-
-        def arrive(i):
-            dev = behind(z, i)
-            copy_of(outgoing, incoming, out_sems, z * per + i, dev, dev, dev).wait_recv()
-
-        each(z, arrive)
-        xs[...] = incoming[pl.ds(c * per, per)].reshape(rows_in, width)
+    def by_distance(k):
+        found = my_z
+        for z in range(nz):
+            inner = 1 if 2 * z < nz - 1 else -1
+            near = sorted(range(nz), key=lambda s: (abs(s - z), -(s - z) * inner))
+            for place in range(nz):
+                found = jnp.where((my_z == z) & (k == place), near[place], found)
+        return found
+
+    def plane_copy(src, dst, sems, z, p, q_to, q_src, q_dst):
+        return pltpu.make_async_remote_copy(
+            src_ref=src.at[z, p, q_src],
+            dst_ref=dst.at[z, p, q_dst],
+            send_sem=sems[0].at[z, p],
+            recv_sem=sems[1].at[z, p],
+            device_id=device(my_z, q_to),
+            device_id_type=MESH,
+        )
+
+    def plane_send(src, dst, sems, z, p):
+        def one(o, _):
+            q = (my_q + o) % plane
+            plane_copy(src, dst, sems, z, p, q, q, my_q).start()
+            return 0
+
+        lax.fori_loop(1, plane, one, 0)
+        dst[z, p, my_q] = src[z, p, my_q]
+
+    def plane_all(src, dst, sems, z, p):
+        others = pl.ds(0, plane - 1)
+        return pltpu.make_async_remote_copy(
+            src_ref=src.at[z, p, others],
+            dst_ref=dst.at[z, p, others],
+            send_sem=sems[0].at[z, p],
+            recv_sem=sems[1].at[z, p],
+            device_id=device(my_z, (my_q + 1) % plane),
+            device_id_type=MESH,
+        )
+
+    out_way = (outgoing, incoming, (out_send, out_recv))
+    back_way = (produced, returned, (back_send, back_recv))
+
+    def dispatch(k):
+        z = by_distance(k)
+
+        def piece(p, _):
+            @pl.when(k > 0)
+            def _():
+                line_copy(z, p, above, up_send).wait_recv()
+                spread(z, p)
+
+            block = jnp.dot(table_t[z], line[z, p], preferred_element_type=jnp.float32)
+            outgoing[z, p] = block.astype(jnp.bfloat16).reshape(plane, cap, part)
+            plane_send(*out_way, z, p)
+            return 0
+
+        lax.fori_loop(0, PARTS, piece, 0)
+
+    def expert(k):
+        z = by_distance(k)
+
+        def arrive(p, _):
+            plane_all(*out_way, z, p).wait_recv()
+            return 0
+
+        lax.fori_loop(0, PARTS, arrive, 0)
 
         def up_tile(t, _):
             at = pl.ds(pl.multiple_of(t * FF_TILE, FF_TILE), FF_TILE)
-            x = xs[...]
+            x = jnp.concatenate(
+                [incoming[z, p].reshape(rows_in, part) for p in range(PARTS)], axis=1
+            )
             a = jnp.dot(x, gate_ref[0, :, at], preferred_element_type=jnp.float32)
             u = jnp.dot(x, up_ref[0, :, at], preferred_element_type=jnp.float32)
             hs[:, at] = (jax.nn.silu(a) * u).astype(jnp.bfloat16)
@@ -370,55 +447,123 @@
 
         lax.fori_loop(0, ff // FF_TILE, up_tile, 0)
 
-        def down_tile(t, _):
-            at = pl.ds(pl.multiple_of(t * FF_TILE, FF_TILE), FF_TILE)
+        def down_tile(p, _):
+            at = pl.ds(pl.multiple_of(p * part, part), part)
             y = jnp.dot(hs[...], down_ref[0, :, at], preferred_element_type=jnp.float32)
-            produced[pl.ds(c * per, per), :, at] = y.astype(jnp.bfloat16).reshape(
-                per, cap, FF_TILE
-            )
+            produced[z, p] = y.astype(jnp.bfloat16).reshape(plane, cap, part)
+            plane_send(*back_way, z, p)
             return 0
 
-        lax.fori_loop(0, width // FF_TILE, down_tile, 0)
-
-        def start(i):
-            dev = behind(z, i)
-            copy_of(produced, returned, back_sems, z * per + i, dev, dev, mine).start()
-
-        each(z, start)
+        lax.fori_loop(0, PARTS, down_tile, 0)
+
+    def partial_copy(z, p):
+        to = jnp.where(z < my_z, below, above)
+        slot = jnp.where((z > my_z) & (to == z), nz, z)
+        return pltpu.make_async_remote_copy(
+            src_ref=partial_out.at[z, p],
+            dst_ref=partial_in.at[slot, p],
+            send_sem=part_send.at[z, p],
+            recv_sem=part_recv.at[slot, p],
+            device_id=device(to, my_q),
+            device_id_type=MESH,
+        )
+
+    def partial_arrive(slot, p):
+        pltpu.make_async_remote_copy(
+            src_ref=partial_out.at[0, p],
+            dst_ref=partial_in.at[slot, p],
+            send_sem=part_send.at[0, p],
+            recv_sem=part_recv.at[slot, p],
+            device_id=device(above, my_q),
+            device_id_type=MESH,
+        ).wait_recv()
+
+    def combine(z, p):
+        plane_all(*back_way, z, p).wait_recv()
+        block = returned[z, p].reshape(rows_in, part)
+        mine = jnp.dot(table_hi[z], block, preferred_element_type=jnp.float32) + jnp.dot(
+            table_lo[z], block, preferred_element_type=jnp.float32
+        )
+        total[PARTS] = mine
+
+        @pl.when(z == my_z)
+        def _():
+            total[p] += total[PARTS]
+
+        @pl.when(z != my_z)
+        def _():
+            @pl.when(~edge)
+            def _():
+                partial_arrive(z, p)
+                total[PARTS] += partial_in[z, p].astype(jnp.float32)
+
+            partial_out[z, p] = total[PARTS].astype(jnp.bfloat16)
+            partial_copy(z, p).start()
+
+    def tick(t, _):
+        @pl.when(t < nz)
+        def _():
+            dispatch(t)
+
+        e = jnp.where(edge | (t == 0), t, t - 1)
+
+        @pl.when((e < nz) & (edge | (t != 1)))
+        def _():
+            expert(e)
+
+        c = jnp.where(edge, t, t - nz)
+
+        @pl.when((c >= 0) & (c < nz))
+        def _():
+            def one(j, _):
+                late = max(nz - 2, 1)
+                m = jnp.maximum(c * PARTS + j - 2 * PARTS, 0)
+                straight = edge | (c < 2)
+                k = jnp.where(straight, c, nz - 1 - m % late)
+                p = jnp.where(straight, j, m // late)
+                combine(by_distance(k), p)
+                return 0
+
+            lax.fori_loop(0, PARTS, one, 0)
+
         return 0
 
-    lax.fori_loop(0, CHUNKS, expert, 0)
-    returned[mine] = produced[mine]
-
-    def combine(turn, _):
-        z = (turn + 1) % CHUNKS
-        c = (my_chunk + z) % CHUNKS
-
-        def arrive(i):
-            dev = ahead(z, i)
-            copy_of(produced, returned, back_sems, z * per + i, dev, dev, dev).wait_recv()
-
-        each(z, arrive)
-        block = returned[pl.ds(c * per, per)].reshape(rows_in, width)
-        proj[...] += route_0 * jnp.dot(
-            table_0[c], block, preferred_element_type=jnp.float32
-        ) + route_1 * jnp.dot(table_1[c], block, preferred_element_type=jnp.float32)
+    lax.fori_loop(0, 2 * nz, tick, 0)
+    for p in range(PARTS):
+        @pl.when(has_above)
+        def _():
+            partial_arrive(my_z, p)
+            total[p] += partial_in[my_z, p].astype(jnp.float32)
+
+        @pl.when(has_below)
+        def _():
+            partial_arrive(nz, p)
+            total[p] += partial_in[nz, p].astype(jnp.float32)
+
+        out_ref[0, :, p * part : (p + 1) * part] = total[p].astype(jnp.bfloat16)
+
+    def drain(i, _):
+        z, p = i // PARTS, i % PARTS
+        plane_all(*out_way, z, p).wait_send()
+        plane_all(*back_way, z, p).wait_send()
+
+        @pl.when((z <= my_z) & has_above)
+        def _():
+            line_copy(z, p, above, up_send).wait_send()
+
+        @pl.when((z >= my_z) & has_below)
+        def _():
+            line_copy(z, p, below, down_send).wait_send()
+
+        @pl.when(z != my_z)
+        def _():
+            partial_copy(z, p).wait_send()
+
         return 0
 
-    lax.fori_loop(0, CHUNKS, combine, 0)
-    out_ref[0] = proj[...].astype(jnp.bfloat16)
-
-    def drain(z, _):
-        def left(i):
-            dev = ahead(z, i)
-            copy_of(outgoing, incoming, out_sems, z * per + i, dev, dev, mine).wait_send()
-            dev = behind(z, i)
-            copy_of(produced, returned, back_sems, z * per + i, dev, dev, mine).wait_send()
-
-        each(z, left)
-        return 0
-
-    lax.fori_loop(0, CHUNKS, drain, 0)
+    lax.fori_loop(0, nz * PARTS, drain, 0)
+    for o in range(1, nz):
+        meta_copy((my_z + o) % nz, my_z).wait_send()
     for o in range(1, n):
         qkv_copy(o).wait_send()
         mixed_copy(o, me).wait_send()
@@ -454,8 +599,10 @@
     tok, width = residual_input.shape[1:]
     dk, dv = queries.shape[2] // n, values.shape[2] // n
     length, devices, ff = n * tok, n * dpn, gate_weight.shape[2]
-    cap, per = 4 * tok // devices, devices // CHUNKS
-    rows_in = per * cap
+    cap, chips = 4 * tok // devices, dpn // 2
+    ny = chips if n % chips == 0 else 1
+    nz, plane = n // ny, ny * dpn
+    rows_in, part = plane * cap, width // PARTS
     operands = (
         queries, keys, values, gate_logits, retention_offset, log_forget_extra,
         lane_amplifier.reshape(1, dv), output_gate_logits, output_projection,
@@ -481,22 +628,28 @@
             pltpu.VMEM((n, tok, dv), bf16),
             pltpu.VMEM((dpn,) + output_projection.shape, bf16),
             pltpu.VMEM((tok, width), f32),
-            pltpu.VMEM((tok, width), bf16),
-            pltpu.VMEM((CHUNKS, rows_in, tok), bf16),
-            pltpu.VMEM((CHUNKS, tok, rows_in), bf16),
-            pltpu.VMEM((CHUNKS, tok, rows_in), bf16),
-            pltpu.VMEM((devices, cap, width), bf16),
-            pltpu.VMEM((devices, cap, width), bf16),
-            pltpu.VMEM((rows_in, width), bf16),
+            pltpu.VMEM((nz, 8, tok), f32),
+            pltpu.VMEM((nz, rows_in, tok), bf16),
+            pltpu.VMEM((nz, tok, rows_in), bf16),
+            pltpu.VMEM((nz, tok, rows_in), bf16),
+            pltpu.VMEM((nz, PARTS, tok, part), bf16),
+            pltpu.VMEM((nz, PARTS, plane, cap, part), bf16),
+            pltpu.VMEM((nz, PARTS, plane, cap, part), bf16),
             pltpu.VMEM((rows_in, ff), bf16),
-            pltpu.VMEM((devices, cap, width), bf16),
-            pltpu.VMEM((devices, cap, width), bf16),
+            pltpu.VMEM((nz, PARTS, plane, cap, part), bf16),
+            pltpu.VMEM((nz, PARTS, plane, cap, part), bf16),
+            pltpu.VMEM((nz, PARTS, tok, part), bf16),
+            pltpu.VMEM((nz + 1, PARTS, tok, part), bf16),
+            pltpu.VMEM((PARTS + 1, tok, part), f32),
             dma((len(operands),)),
             dma((n,)), dma((n,)), dma((n,)), dma((n,)),
             dma((dpn // 2, PIECES)), dma((dpn // 2, PIECES)),
             dma((dpn // 2, PIECES)), dma((dpn // 2, PIECES)),
             dma(()),
-            dma((devices,)), dma((devices,)), dma((devices,)), dma((devices,)),
+            dma((nz,)), dma((nz,)),
+            dma((nz, PARTS)), dma((nz, PARTS)), dma((nz, PARTS)),
+            dma((nz, PARTS)), dma((nz, PARTS)), dma((nz, PARTS)), dma((nz, PARTS)),
+            dma((nz, PARTS)), dma((nz + 1, PARTS)),
         ],
         compiler_params=pltpu.CompilerParams(
             collective_id=0, has_side_effects=True, vmem_limit_bytes=60 * 1024 * 1024

time: 147 us -> 141 us (0.959)
  Pallas kernels: 139 us -> 134 us
    pallas_call x1, Pallas kernels: 139 us -> 134 us  [on_device(): pl.pallas_call(partial(layer_kernel, n=n, dpn=dpn, inputs=len(operands)),...]
where the time goes in v1:
time: 141 us
  Pallas kernels  134 us (95%)
  local copies, waits for them, and re-layouts  7.5 us (5%)
    pallas_call x1, Pallas kernels, on_device(): pl.pallas_call(partial(layer_kernel, n=n, dpn=dpn, inputs=len(operands)),...  134 us
    unnamed x5, local copies, waits for them, and re-layouts  7.5 us

profile of v1, /device:TPU:0, one launch (start us, length us, event | category | flops | bytes accessed | tf_op | source)
XLA Modules:
  0.0 141.2 jit_solution(2420422571773516624)
XLA Ops:
  0.0 1.4 copy.19.refs_3_
  1.4 1.4 %copy.20.refs_12_ = s32[1,128,2]{2,1,0:T(8,128)} copy(s32[1,128,2]{1,2,0:T(2,128)} %param.30) | data formatting | bytes 2048 | tf_op args[12]
  2.8 1.4 copy.21.refs_13_
  4.2 1.4 copy.22.refs_14_
  5.6 133.7 %shard_map.172 = bf16[1,128,2048]{2,1,0:T(8,128)(2,1)} custom-call(bf16[1,128,512]{2,1,0:T(8,128)(2,1)} %refs_0_.1, bf16[1,128,512]{2,1,0:T(8,128)(2,1)} %refs_1_.1, bf16[1,128,1024]{2,1,0:T(8,128)(2,1)} %refs_2_.1, bf16[1,128,32]{2,1,0:T(8,128)(2,1)} %copy.19.refs_3_, f32[1,2]{1,0:T(1,128)} %refs_4_.1, f32[1,1,1024]{2,1,0:T(1,128)} %refs_5_.1, ...), custom_call_target="tpu_custom_call" | custom-call | tf_op jit(solution)/shard_map/pallas_call | solution.py:616
  139.4 1.9 %copy.24 = bf16[1,128,2048]{2,1,0:T(8,128)(2,1)} copy(bf16[1,128,2048]{2,1,0:T(8,128)(2,1)} %shard_map.172) | data formatting | bytes 1048576

commit v2 on v1

--- a/solution.py
+++ b/solution.py
@@ -12,7 +12,7 @@
 GATE_ROWS = 16
 PARTS = 4
 FF_TILE = 256
-PIECES = 4
+PIECES = 8
 
 
 def log_sigmoid(x):
@@ -31,13 +31,14 @@
         send, recv, gates_t, cols, mixed, mrecv, wfull, proj,
         meta, table_t, table_hi, table_lo, line, outgoing, incoming, hs, produced, returned,
         partial_out, partial_in, total,
-        in_sem, send_sem, recv_sem, msend_sem, mrecv_sem, wx_send, wx_recv, wc_send, wc_recv,
-        wl_sem, meta_send, meta_recv, up_send, down_send, line_recv,
+        in_sem, send_sem, recv_sem, msend_sem, mrecv_sem, wx_send, wx_recv, wy_send, wc_send,
+        wc_recv, wl_sem, meta_send, meta_recv, up_send, down_send, line_recv,
         out_send, out_recv, back_send, back_recv, part_send, part_recv,
     ) = rest
     loads = [pltpu.make_async_copy(hbm[i], local[i], in_sem.at[i]) for i in range(inputs)]
-    for load in loads:
-        load.start()
+    early = (0, 1, 2, 3, 8)
+    for i in early:
+        loads[i].start()
     tok = q_ref.shape[1]
     dk = q_ref.shape[2] // n
     dv = v_ref.shape[2] // n
@@ -82,9 +83,9 @@
         send[h, 0:tok, 0:dk] = k_ref[0, :, h * dk : (h + 1) * dk]
         send[h, 0:tok, dk : 2 * dk] = q_ref[0, :, h * dk : (h + 1) * dk]
         send[h, 0:tok, 2 * dk : 2 * dk + dv] = v_ref[0, :, h * dv : (h + 1) * dv]
-    g = g_ref[0].astype(jnp.float32)
-    g = jnp.concatenate([g, jnp.zeros((tok, 128 - g.shape[1]), jnp.float32)], axis=1)
-    gates_t[...] = g.T
+    gate_rows = g_ref.shape[1]
+    gates_t[0:gate_rows] = g_ref[0].astype(jnp.float32)
+    gates_t[gate_rows:] = jnp.zeros((128 - gate_rows, tok), jnp.float32)
     for h in range(n):
         send[h, tok : tok + GATE_ROWS, 0:tok] = gates_t[4 * h : 4 * h + GATE_ROWS, :].astype(
             jnp.bfloat16
@@ -94,6 +95,9 @@
         )
 
     pl.semaphore_wait(barrier, n - 1 + plane - 1)
+    for i in range(inputs):
+        if i not in early:
+            loads[i].start()
 
     def qkv_copy(o):
         return pltpu.make_async_remote_copy(
@@ -117,42 +121,71 @@
 
     piece = w_ref.shape[0] // PIECES
 
-    def wx_copy(o, p, slot):
-        return pltpu.make_async_remote_copy(
-            src_ref=w_ref.at[pl.ds(p * piece, piece)],
-            dst_ref=wfull.at[slot, pl.ds(p * piece, piece)],
+    share = PIECES // ny
+    first_piece = my_y * share
+
+    def rows_of(p):
+        return pl.ds(pl.multiple_of(p * piece, piece), piece)
+
+    def wx_copy(o, p):
+        return pltpu.make_async_remote_copy(
+            src_ref=w_ref.at[rows_of(p)],
+            dst_ref=wfull.at[my_dp, rows_of(p)],
             send_sem=wx_send.at[o, p],
             recv_sem=wx_recv.at[o, p],
             device_id={"sp": me, "dp": ((my_x + o) % chips) * 2 + my_core},
             device_id_type=MESH,
         )
 
-    def wc_copy(o, p, src, slot):
-        return pltpu.make_async_remote_copy(
-            src_ref=src.at[pl.ds(p * piece, piece)],
-            dst_ref=wfull.at[slot, pl.ds(p * piece, piece)],
+    def from_chip(o):
+        return ((my_x + chips - o) % chips) * 2 + my_core
+
+    def wy_copy(o, p, yo):
+        return pltpu.make_async_remote_copy(
+            src_ref=wfull.at[from_chip(o), rows_of(p)],
+            dst_ref=wfull.at[from_chip(o), rows_of(p)],
+            send_sem=wy_send.at[o, p, yo],
+            recv_sem=wx_recv.at[o, p],
+            device_id={"sp": my_z * ny + (my_y + yo) % ny, "dp": my_dp},
+            device_id_type=MESH,
+        )
+
+    def wc_copy(o, p):
+        return pltpu.make_async_remote_copy(
+            src_ref=wfull.at[from_chip(o), rows_of(p)],
+            dst_ref=wfull.at[from_chip(o), rows_of(p)],
             send_sem=wc_send.at[o, p],
             recv_sem=wc_recv.at[o, p],
             device_id={"sp": me, "dp": my_x * 2 + 1 - my_core},
             device_id_type=MESH,
         )
 
-    def from_chip(o):
-        return ((my_x + chips - o) % chips) * 2 + my_core
-
-    def pass_on(p):
+    def own_copy():
+        return pltpu.make_async_remote_copy(
+            src_ref=w_ref,
+            dst_ref=wfull.at[my_dp],
+            send_sem=wc_send.at[0, 0],
+            recv_sem=wc_recv.at[0, 0],
+            device_id={"sp": me, "dp": my_x * 2 + 1 - my_core},
+            device_id_type=MESH,
+        )
+
+    def pass_on(j):
+        p = (first_piece + j) % PIECES
         for o in range(1, chips):
-            slot = from_chip(o)
-            wx_copy(o, p, slot).wait_recv()
-            wc_copy(o, p, wfull.at[slot], slot).start()
+            wx_copy(o, p).wait_recv()
+            wc_copy(o, p).start()
+            if j < share:
+                for yo in range(1, ny):
+                    wy_copy(o, p, yo).start()
 
     for o in range(1, n):
         qkv_copy(o).start()
     loads[8].wait()
-    for p in range(PIECES):
+    for j in range(share):
         for o in range(1, chips):
-            wx_copy(o, p, my_dp).start()
-        wc_copy(0, p, w_ref, my_dp).start()
+            wx_copy(o, first_piece + j).start()
+    own_copy().start()
     own_w = pltpu.make_async_copy(w_ref, wfull.at[my_dp], wl_sem)
     own_w.start()
     recv[me] = send[me]
@@ -161,37 +194,38 @@
 
     rows_in = plane * cap
     ids = index_ref[0].astype(jnp.float32)
-    e_0, e_1 = ids[:, 0:1], ids[:, 1:2]
+    e_0, e_1 = ids[0:1], ids[1:2]
     wide = -(-devices // 128) * 128
-    lane_e = lax.broadcasted_iota(jnp.int32, (tok, wide), 1).astype(jnp.float32)
-    hit_0 = jnp.where(lane_e == e_0, 1.0, 0.0)
-    hit_1 = jnp.where(lane_e == e_1, 1.0, 0.0)
+    sub_e = lax.broadcasted_iota(jnp.int32, (wide, tok), 0).astype(jnp.float32)
+    hit_0 = jnp.where(sub_e == e_0, 1.0, 0.0)
+    hit_1 = jnp.where(sub_e == e_1, 1.0, 0.0)
     tri = jnp.where(
-        lax.broadcasted_iota(jnp.int32, (tok, tok), 1)
-        < lax.broadcasted_iota(jnp.int32, (tok, tok), 0),
+        lax.broadcasted_iota(jnp.int32, (tok, tok), 0)
+        < lax.broadcasted_iota(jnp.int32, (tok, tok), 1),
         1.0,
         0.0,
     ).astype(jnp.bfloat16)
-    rank_0 = jnp.dot(tri, hit_0.astype(jnp.bfloat16), preferred_element_type=jnp.float32)
-    rank_1 = jnp.dot(tri, hit_1.astype(jnp.bfloat16), preferred_element_type=jnp.float32)
-    rank_1 = rank_1 + jnp.sum(hit_0, axis=0, keepdims=True)
-    place_0 = e_0 * cap + jnp.sum(hit_0 * rank_0, axis=1, keepdims=True)
-    place_1 = e_1 * cap + jnp.sum(hit_1 * rank_1, axis=1, keepdims=True)
-    groups = group_ref.shape[2]
+    rank_0 = jnp.dot(hit_0.astype(jnp.bfloat16), tri, preferred_element_type=jnp.float32)
+    rank_1 = jnp.dot(hit_1.astype(jnp.bfloat16), tri, preferred_element_type=jnp.float32)
+    rank_1 = rank_1 + jnp.sum(hit_0, axis=1, keepdims=True)
+    place_0 = e_0 * cap + jnp.sum(hit_0 * rank_0, axis=0, keepdims=True)
+    place_1 = e_1 * cap + jnp.sum(hit_1 * rank_1, axis=0, keepdims=True)
+    groups = group_ref.shape[1]
     span = devices // groups
-    route_0 = jnp.zeros((tok, 1), jnp.float32)
-    route_1 = jnp.zeros((tok, 1), jnp.float32)
+    route_0 = jnp.zeros((1, tok), jnp.float32)
+    route_1 = jnp.zeros((1, tok), jnp.float32)
     for c in range(groups):
-        weight_c = group_ref[0, :, c : c + 1]
+        weight_c = group_ref[0, c : c + 1, :]
         route_0 += jnp.where((e_0 >= c * span) & (e_0 < (c + 1) * span), weight_c, 0.0)
         route_1 += jnp.where((e_1 >= c * span) & (e_1 < (c + 1) * span), weight_c, 0.0)
-    route_0 = route_0 * within_ref[0, :, 0:1]
-    route_1 = route_1 * within_ref[0, :, 1:2]
-    lane_t = lax.broadcasted_iota(jnp.int32, (tok, 128), 1)
-    packed = jnp.where(
-        lane_t == 0, place_0, jnp.where(lane_t == 1, place_1, jnp.where(lane_t == 2, route_0, route_1))
+    route_0 = route_0 * within_ref[0, 0:1, :]
+    route_1 = route_1 * within_ref[0, 1:2, :]
+    sub_m = lax.broadcasted_iota(jnp.int32, (8, tok), 0)
+    meta[my_z] = jnp.where(
+        sub_m == 0,
+        place_0,
+        jnp.where(sub_m == 1, place_1, jnp.where(sub_m == 2, route_0, route_1)),
     )
-    meta[my_z] = packed.T[0:8]
 
     def meta_copy(z, slot):
         return pltpu.make_async_remote_copy(
@@ -206,6 +240,8 @@
     for o in range(1, nz):
         meta_copy((my_z + o) % nz, my_z).start()
 
+    for j in range(max(share - 1, 1)):
+        pass_on(j)
     for o in range(1, n):
         qkv_arrival(o).wait_recv()
 
@@ -277,16 +313,21 @@
         def _():
             mixed_copy(j, me).start()
 
+        @pl.when(j == 0)
+        def _():
+            for late in range(max(share - 1, 1), share):
+                pass_on(late)
+
         @pl.when(j == n // 2)
         def _():
-            pass_on(PIECES - 2)
+            for late in range(share, share + (PIECES - share) // 2):
+                pass_on(late)
 
         return 0
 
-    for p in range(PIECES - 2):
-        pass_on(p)
     lax.fori_loop(0, n, segment, 0)
-    pass_on(PIECES - 1)
+    for j in range(share + (PIECES - share) // 2, PIECES):
+        pass_on(j)
     mrecv[me] = mixed[me]
     sub_r = lax.broadcasted_iota(jnp.int32, (rows_in, tok), 0).astype(jnp.float32)
     at = sub_r + (my_z * rows_in).astype(jnp.float32)
@@ -314,12 +355,10 @@
     gated = jnp.concatenate([mrecv[h].astype(jnp.float32) for h in range(n)], axis=1) * sig
     gated = gated.astype(jnp.bfloat16)
     own_w.wait()
-    partner = 1 - my_core
+    own_copy().wait_recv()
     for p in range(PIECES):
-        wc_copy(0, p, w_ref, my_x * 2 + partner).wait_recv()
         for o in range(1, chips):
-            slot = ((my_x + chips - o) % chips) * 2 + partner
-            wc_copy(o, p, wfull.at[slot], slot).wait_recv()
+            wc_copy(o, p).wait_recv()
     for j in range(dpn):
         proj[:, j * wcol : (j + 1) * wcol] = jnp.dot(
             gated, wfull[j], preferred_element_type=jnp.float32
@@ -410,7 +449,7 @@
     out_way = (outgoing, incoming, (out_send, out_recv))
     back_way = (produced, returned, (back_send, back_recv))
 
-    def dispatch(k):
+    def dispatch(k, first, last):
         z = by_distance(k)
 
         def piece(p, _):
@@ -424,9 +463,9 @@
             plane_send(*out_way, z, p)
             return 0
 
-        lax.fori_loop(0, PARTS, piece, 0)
-
-    def expert(k):
+        lax.fori_loop(first, last, piece, 0)
+
+    def expert(k, inline):
         z = by_distance(k)
 
         def arrive(p, _):
@@ -451,10 +490,21 @@
             at = pl.ds(pl.multiple_of(p * part, part), part)
             y = jnp.dot(hs[...], down_ref[0, :, at], preferred_element_type=jnp.float32)
             produced[z, p] = y.astype(jnp.bfloat16).reshape(plane, cap, part)
-            plane_send(*back_way, z, p)
+
+            @pl.when(inline)
+            def _():
+                plane_send(*back_way, z, p)
+
             return 0
 
         lax.fori_loop(0, PARTS, down_tile, 0)
+
+    def send_back(k):
+        def piece(p, _):
+            plane_send(*back_way, by_distance(k), p)
+            return 0
+
+        lax.fori_loop(0, PARTS, piece, 0)
 
     def partial_copy(z, p):
         to = jnp.where(z < my_z, below, above)
@@ -500,35 +550,57 @@
             partial_out[z, p] = total[PARTS].astype(jnp.bfloat16)
             partial_copy(z, p).start()
 
-    def tick(t, _):
-        @pl.when(t < nz)
-        def _():
-            dispatch(t)
-
-        e = jnp.where(edge | (t == 0), t, t - 1)
-
-        @pl.when((e < nz) & (edge | (t != 1)))
-        def _():
-            expert(e)
-
-        c = jnp.where(edge, t, t - nz)
-
-        @pl.when((c >= 0) & (c < nz))
-        def _():
-            def one(j, _):
-                late = max(nz - 2, 1)
-                m = jnp.maximum(c * PARTS + j - 2 * PARTS, 0)
-                straight = edge | (c < 2)
-                k = jnp.where(straight, c, nz - 1 - m % late)
-                p = jnp.where(straight, j, m // late)
-                combine(by_distance(k), p)
-                return 0
-
-            lax.fori_loop(0, PARTS, one, 0)
+    def combine_all(k):
+        def one(p, _):
+            combine(by_distance(k), p)
+            return 0
+
+        lax.fori_loop(0, PARTS, one, 0)
+
+    dispatch(0, 0, PARTS)
+    half = PARTS // 2
+
+    def tick(k, _):
+        last = k == nz - 1
+        stop = jnp.where(last, 0, PARTS)
+        early = jnp.minimum(jnp.where(k == 0, half, jnp.where(edge, jnp.where(k == 1, half // 2, half), PARTS)), stop)
+        dispatch(k + 1, 0, early)
+
+        @pl.when(~edge & (k == nz - 2))
+        def _():
+            send_back(1)
+
+        expert(k, edge & (k > 0))
+        dispatch(k + 1, early, stop)
+
+        @pl.when(edge & (k > 0))
+        def _():
+            combine_all(k)
 
         return 0
 
-    lax.fori_loop(0, 2 * nz, tick, 0)
+    lax.fori_loop(0, nz, tick, 0)
+
+    @pl.when(edge)
+    def _():
+        send_back(0)
+
+    @pl.when(~edge)
+    def _():
+        for k in range(nz - 1, 1, -1):
+            send_back(k)
+        send_back(0)
+        if nz > 2:
+            combine_all(1)
+        late = max(nz - 2, 1)
+
+        def one(m, _):
+            combine(by_distance(nz - 1 - m % late), m // late)
+            return 0
+
+        lax.fori_loop(0, (nz - 2) * PARTS, one, 0)
+
+    combine_all(0)
     for p in range(PARTS):
         @pl.when(has_above)
         def _():
@@ -567,12 +639,14 @@
     for o in range(1, n):
         qkv_copy(o).wait_send()
         mixed_copy(o, me).wait_send()
-    for p in range(PIECES):
-        for o in range(1, chips):
-            wx_copy(o, p, my_dp).wait_send()
-            slot = from_chip(o)
-            wc_copy(o, p, wfull.at[slot], slot).wait_send()
-        wc_copy(0, p, w_ref, my_dp).wait_send()
+    own_copy().wait_send()
+    for o in range(1, chips):
+        for p in range(PIECES):
+            wc_copy(o, p).wait_send()
+        for j in range(share):
+            wx_copy(o, first_piece + j).wait_send()
+            for yo in range(1, ny):
+                wy_copy(o, first_piece + j, yo).wait_send()
 
 
 def on_device(
@@ -604,10 +678,11 @@
     nz, plane = n // ny, ny * dpn
     rows_in, part = plane * cap, width // PARTS
     operands = (
-        queries, keys, values, gate_logits, retention_offset, log_forget_extra,
+        queries, keys, values, jnp.swapaxes(gate_logits, 1, 2), retention_offset, log_forget_extra,
         lane_amplifier.reshape(1, dv), output_gate_logits, output_projection,
         residual_input, cell_norm_gain.reshape(1, width), expert_norm_gain.reshape(1, width),
-        expert_index, group_mixing_weight, within_group_weight,
+        jnp.swapaxes(expert_index, 1, 2), jnp.swapaxes(group_mixing_weight, 1, 2),
+        jnp.swapaxes(within_group_weight, 1, 2),
         gate_weight, up_weight, down_weight,
     )
     dma = pltpu.SemaphoreType.DMA
@@ -615,7 +690,7 @@
     hbm = pl.BlockSpec(memory_space=pltpu.HBM)
     return pl.pallas_call(
         partial(layer_kernel, n=n, dpn=dpn, inputs=len(operands)),
-        out_shape=jax.ShapeDtypeStruct((1, tok, width), bf16),
+        out_shape=pltpu.VMEM((1, tok, width), bf16),
         in_specs=[hbm] * len(operands),
         out_specs=pl.BlockSpec(memory_space=pltpu.VMEM),
         scratch_shapes=[pltpu.VMEM(x.shape, x.dtype) for x in operands]
@@ -643,8 +718,8 @@
             pltpu.VMEM((PARTS + 1, tok, part), f32),
             dma((len(operands),)),
             dma((n,)), dma((n,)), dma((n,)), dma((n,)),
-            dma((dpn // 2, PIECES)), dma((dpn // 2, PIECES)),
-            dma((dpn // 2, PIECES)), dma((dpn // 2, PIECES)),
+            dma((chips, PIECES)), dma((chips, PIECES)), dma((chips, PIECES, ny)),
+            dma((chips, PIECES)), dma((chips, PIECES)),
             dma(()),
             dma((nz,)), dma((nz,)),
             dma((nz, PARTS)), dma((nz, PARTS)), dma((nz, PARTS)),

time: 141 us -> 114 us (0.81)
  Pallas kernels: 134 us -> 113 us
  local copies, waits for them, and re-layouts: 7.5 us -> 0.8 us
    pallas_call x1, Pallas kernels: 134 us -> 113 us  [on_device(): pl.pallas_call(partial(layer_kernel, n=n, dpn=dpn, inputs=len(operands)),...]
    unnamed x5 -> x1, local copies, waits for them, and re-layouts: 7.5 us -> 0.8 us
where the time goes in v2:
time: 114 us
  Pallas kernels  113 us (99%)
    pallas_call x1, Pallas kernels, on_device(): pl.pallas_call(partial(layer_kernel, n=n, dpn=dpn, inputs=len(operands)),...  113 us

profile of v2, /device:TPU:0, one launch (start us, length us, event | category | flops | bytes accessed | tf_op | source)
XLA Modules:
  0.0 114.1 jit_solution(6633736523197782537)
XLA Ops:
  0.0 113.3 %shard_map.172 = bf16[1,128,2048]{2,1,0:T(8,128)(2,1)S(1)} custom-call(bf16[1,128,512]{2,1,0:T(8,128)(2,1)} %refs_0_.1, bf16[1,128,512]{2,1,0:T(8,128)(2,1)} %refs_1_.1, bf16[1,128,1024]{2,1,0:T(8,128)(2,1)} %refs_2_.1, bf16[1,32,128]{2,1,0:T(8,128)(2,1)} %bitcast.7, f32[1,2]{1,0:T(1,128)} %refs_4_.1, f32[1,1,1024]{2,1,0:T(1,128)} %refs_5_.1, ...), custom_call_target="tpu_custom_call" | custom-call | tf_op jit(solution)/shard_map/pallas_call | solution.py:691
  113.3 0.8 copy.20

commit v3 on v2

--- a/solution.py
+++ b/solution.py
@@ -11,8 +11,10 @@
 MESH = pl.DeviceIdType.MESH
 GATE_ROWS = 16
 PARTS = 4
+SUBS = 2
 FF_TILE = 256
 PIECES = 8
+EXTRA = 1
 
 
 def log_sigmoid(x):
@@ -28,10 +30,11 @@
         gate_ref, up_ref, down_ref,
     ) = local
     (
-        send, recv, gates_t, cols, mixed, mrecv, wfull, proj,
+        send, recv, gates_t, params, rows_of_gate, cols, weights, sums, state_out, state_in,
+        mixed, mrecv, wfull, proj,
         meta, table_t, table_hi, table_lo, line, outgoing, incoming, hs, produced, returned,
         partial_out, partial_in, total,
-        in_sem, send_sem, recv_sem, msend_sem, mrecv_sem, wx_send, wx_recv, wy_send, wc_send,
+        in_sem, send_sem, recv_sem, param_send, param_recv, state_send, state_recv, msend_sem, mrecv_sem, wx_send, wx_recv, wy_send, wc_send,
         wc_recv, wl_sem, meta_send, meta_recv, up_send, down_send, line_recv,
         out_send, out_recv, back_send, back_recv, part_send, part_recv,
     ) = rest
@@ -42,9 +45,13 @@
     tok = q_ref.shape[1]
     dk = q_ref.shape[2] // n
     dv = v_ref.shape[2] // n
-    length = n * tok
+    half = n // 2
+    length = half * tok
     wcol = w_ref.shape[1]
     me = lax.axis_index("sp")
+    my_half, my_rank = me // half, me % half
+    first = my_half * half
+    opposite = (me + half) % n
     my_dp = lax.axis_index("dp")
     my_x, my_core = my_dp // 2, my_dp % 2
     chips = dpn // 2
@@ -99,29 +106,50 @@
         if i not in early:
             loads[i].start()
 
-    def qkv_copy(o):
-        return pltpu.make_async_remote_copy(
-            src_ref=send.at[(me + o) % n],
-            dst_ref=recv.at[me],
-            send_sem=send_sem.at[o],
-            recv_sem=recv_sem.at[o],
-            device_id={"sp": (me + o) % n, "dp": my_dp},
-            device_id_type=MESH,
-        )
-
-    def qkv_arrival(o):
-        return pltpu.make_async_remote_copy(
-            src_ref=send.at[(me + o) % n],
-            dst_ref=recv.at[(me + n - o) % n],
-            send_sem=send_sem.at[o],
-            recv_sem=recv_sem.at[o],
-            device_id={"sp": (me + o) % n, "dp": my_dp},
+    def qkv_copy(o, j):
+        return pltpu.make_async_remote_copy(
+            src_ref=send.at[(my_rank + o) % half + j * half],
+            dst_ref=recv.at[j, my_rank],
+            send_sem=send_sem.at[o, j],
+            recv_sem=recv_sem.at[o, j],
+            device_id={"sp": first + (my_rank + o) % half, "dp": my_dp},
+            device_id_type=MESH,
+        )
+
+    def qkv_arrival(o, j):
+        return pltpu.make_async_remote_copy(
+            src_ref=send.at[(my_rank + o) % half + j * half],
+            dst_ref=recv.at[j, (my_rank + half - o) % half],
+            send_sem=send_sem.at[o, j],
+            recv_sem=recv_sem.at[o, j],
+            device_id={"sp": first + (my_rank + o) % half, "dp": my_dp},
+            device_id_type=MESH,
+        )
+
+    def param_copy(slot):
+        return pltpu.make_async_remote_copy(
+            src_ref=params.at[my_half],
+            dst_ref=params.at[slot],
+            send_sem=param_send,
+            recv_sem=param_recv,
+            device_id={"sp": opposite, "dp": my_dp},
+            device_id_type=MESH,
+        )
+
+    def state_copy():
+        return pltpu.make_async_remote_copy(
+            src_ref=state_out,
+            dst_ref=state_in,
+            send_sem=state_send,
+            recv_sem=state_recv,
+            device_id={"sp": opposite, "dp": my_dp},
             device_id_type=MESH,
         )
 
     piece = w_ref.shape[0] // PIECES
 
     share = PIECES // ny
+    direct = share + (EXTRA if ny > 1 else 0)
     first_piece = my_y * share
 
     def rows_of(p):
@@ -170,27 +198,40 @@
             device_id_type=MESH,
         )
 
+    def onward(j, yo):
+        return j < share and (j >= EXTRA or yo < ny - 1)
+
     def pass_on(j):
         p = (first_piece + j) % PIECES
         for o in range(1, chips):
             wx_copy(o, p).wait_recv()
             wc_copy(o, p).start()
-            if j < share:
-                for yo in range(1, ny):
+            for yo in range(1, ny):
+                if onward(j, yo):
                     wy_copy(o, p, yo).start()
 
-    for o in range(1, n):
-        qkv_copy(o).start()
+    for o in range(1, half):
+        for j in range(2):
+            qkv_copy(o, j).start()
     loads[8].wait()
-    for j in range(share):
+    for j in range(direct):
         for o in range(1, chips):
-            wx_copy(o, first_piece + j).start()
+            wx_copy(o, (first_piece + j) % PIECES).start()
     own_copy().start()
     own_w = pltpu.make_async_copy(w_ref, wfull.at[my_dp], wl_sem)
     own_w.start()
-    recv[me] = send[me]
+    for j in range(2):
+        recv[j, my_rank] = send[my_rank + j * half]
     for i in (4, 5, 6, 7, 9, 10, 11, 12, 13, 14):
         loads[i].wait()
+    for d in range(n):
+        params[my_half, d : d + 1, 0:tok] = extra_ref[0, :, d * tok : (d + 1) * tok]
+    params[my_half, n : n + 1, 0:dv] = amp_ref[...]
+    lane_p = lax.broadcasted_iota(jnp.int32, (1, params.shape[2]), 1)
+    params[my_half, n + 1 : n + 2] = jnp.where(
+        lane_p == 0, offset_ref[0:1, 0:1], offset_ref[0:1, 1:2]
+    )
+    param_copy(my_half).start()
 
     rows_in = plane * cap
     ids = index_ref[0].astype(jnp.float32)
@@ -240,95 +281,170 @@
     for o in range(1, nz):
         meta_copy((my_z + o) % nz, my_z).start()
 
-    for j in range(max(share - 1, 1)):
-        pass_on(j)
-    for o in range(1, n):
-        qkv_arrival(o).wait_recv()
-
-    gates = jnp.concatenate(
-        [recv[d, tok : tok + GATE_ROWS, 0:tok].astype(jnp.float32) for d in range(n)], axis=1
-    )
-    extra = extra_ref[0]
-    f = log_sigmoid(gates[1:2] + offset_ref[0:1, 0:1]) + extra
-    b = log_sigmoid(gates[3:4] + offset_ref[0:1, 1:2]) + extra
-    f = jnp.broadcast_to(f, (8, length))
-    b = jnp.broadcast_to(b, (8, length))
+    stops = [PIECES * i // 8 for i in (2, 3, 5, 6, 8)]
+
+    def pass_until(i):
+        for j in range(stops[i - 1] if i else 0, stops[i]):
+            pass_on(j)
+
+    pass_until(0)
+    for o in range(1, half):
+        for j in range(2):
+            qkv_arrival(o, j).wait_recv()
+    param_copy(1 - my_half).wait_recv()
+
+    upper = my_half == 1
     lane = lax.broadcasted_iota(jnp.int32, (8, length), 1)
+    sub = lax.broadcasted_iota(jnp.int32, (8, length), 0)
+    gates, f, b = [], [], []
+    for j in range(2):
+        gates.append(
+            jnp.concatenate(
+                [recv[j, d, tok : tok + GATE_ROWS, 0:tok].astype(jnp.float32) for d in range(half)],
+                axis=1,
+            )
+        )
+        extra = jnp.concatenate(
+            [params[j, pl.ds(first + d, 1), 0:tok] for d in range(half)], axis=1
+        )
+        offset = params[j, n + 1 : n + 2]
+        f.append(log_sigmoid(gates[j][1:2] + offset[:, 0:1]) + extra)
+        b.append(log_sigmoid(gates[j][3:4] + offset[:, 1:2]) + extra)
+    f = jnp.where(sub == 0, f[0], f[1])
+    b = jnp.where(sub == 0, b[0], b[1])
     step = 1
     while step < length:
         f = f + jnp.where(lane >= step, pltpu.roll(f, step, 1), 0.0)
         b = b + jnp.where(lane < length - step, pltpu.roll(b, length - step, 1), 0.0)
         step *= 2
-    row_i = gates[0:1]
-    row_f = row_i - f[0:1]
-    row_b = gates[2:3] - b[0:1]
-    sub = lax.broadcasted_iota(jnp.int32, (128, length), 0)
-    stacked = jnp.where(sub == 0, f[0:1], jnp.where(sub == 1, b[0:1], row_i))
-    cols[...] = stacked.T
+    wide_sub = lax.broadcasted_iota(jnp.int32, (128, length), 0)
+    for j in range(2):
+        row_i = gates[j][0:1]
+        row_f = row_i - f[j : j + 1]
+        row_b = gates[j][2:3] - b[j : j + 1]
+        rows_of_gate[j] = jnp.where(sub == 0, row_f, row_b)
+        leaving = jnp.exp(
+            jnp.where(upper, row_b + b[j : j + 1, 0:1], row_f + f[j : j + 1, length - 1 : length])
+        )
+        stacked = jnp.where(wide_sub == 0, f[j : j + 1], jnp.where(wide_sub == 1, b[j : j + 1], row_i))
+        cols[j] = jnp.where(wide_sub == 3, leaving, stacked).T
 
     scale = dk ** (-0.5)
-    amp = amp_ref[...]
-
-    def mixed_copy(o, slot):
-        return pltpu.make_async_remote_copy(
-            src_ref=mixed.at[(me + o) % n],
-            dst_ref=mrecv.at[slot],
-            send_sem=msend_sem.at[o],
-            recv_sem=mrecv_sem.at[o],
-            device_id={"sp": (me + o) % n, "dp": my_dp},
-            device_id_type=MESH,
-        )
-
-    def segment(j, _):
-        d = (me + 1 + j) % n
+
+    def state(j, _):
+        kq = recv[j, :, 0:tok, 0 : 2 * dk].reshape(length, 2 * dk).astype(jnp.float32)
+        kq = kq * cols[j][:, 3:4]
+        memory = lax.dot_general(
+            kq.astype(jnp.bfloat16),
+            recv[j, :, 0:tok, 2 * dk : 2 * dk + dv].reshape(length, dv),
+            (((0,), (0,)), ((), ())),
+            preferred_element_type=jnp.float32,
+        )
+        normal = jnp.sum(kq, axis=0, keepdims=True)
+        high = normal.astype(jnp.bfloat16).astype(jnp.float32)
+        at = lax.broadcasted_iota(jnp.int32, (GATE_ROWS, 2 * dk), 0)
+        state_out[j, 0:dk] = memory[0:dk].astype(jnp.bfloat16)
+        state_out[j, dk:, 0 : 2 * dk] = jnp.where(
+            at == 0, high, jnp.where(at == 1, normal - high, 0.0)
+        ).astype(jnp.bfloat16)
+        return 0
+
+    lax.fori_loop(0, 2, state, 0)
+    state_copy().start()
+    pass_until(1)
+
+    def mixed_copy(o, j, rank):
+        return pltpu.make_async_remote_copy(
+            src_ref=mixed.at[j, (my_rank + o) % half],
+            dst_ref=mrecv.at[rank + j * half],
+            send_sem=msend_sem.at[o, j],
+            recv_sem=mrecv_sem.at[o, j],
+            device_id={"sp": first + (my_rank + o) % half, "dp": my_dp},
+            device_id_type=MESH,
+        )
+
+    def scaled(j, d):
+        return recv[j, d, 0:tok, dk : 2 * dk].astype(jnp.float32) * scale
+
+    def before_of(d):
+        t_pos = d * tok + lax.broadcasted_iota(jnp.int32, (tok, length), 0)
+        return lax.broadcasted_iota(jnp.int32, (tok, length), 1) < t_pos
+
+    lane_z = lax.broadcasted_iota(jnp.int32, (tok, 128), 1)
+
+    def weigh_head(d, k, j):
+        m = 2 * k + j
         start = pl.multiple_of(d * tok, tok)
-        kq = recv[d, 0:tok, 0 : 2 * dk]
-        qs = kq[:, dk:].astype(jnp.float32) * scale
-        ks = kq[:, :dk].astype(jnp.float32)
+        qs = scaled(j, d)
+        ks = recv[j, d, 0:tok, 0:dk].astype(jnp.float32)
         diag = jnp.sum(qs * ks, axis=1, keepdims=True)
         qs = jnp.concatenate([qs, jnp.zeros_like(qs)], axis=1).astype(jnp.bfloat16)
-        kall = recv[:, 0:tok, 0 : 2 * dk].reshape(length, 2 * dk)
-        vall = recv[:, 0:tok, 2 * dk : 2 * dk + dv].reshape(length, dv)
+        kall = recv[j, :, 0:tok, 0 : 2 * dk].reshape(length, 2 * dk)
         scores = lax.dot_general(
             qs, kall, (((1,), (1,)), ((), ())), preferred_element_type=jnp.float32
         )
-        col = cols[pl.ds(start, tok), :]
+        col = cols[j, pl.ds(start, tok), :]
         col_f, col_b, col_i = col[:, 0:1], col[:, 1:2], col[:, 2:3]
-        t_pos = start + lax.broadcasted_iota(jnp.int32, (tok, length), 0)
-        s_pos = lax.broadcasted_iota(jnp.int32, (tok, length), 1)
-        before = s_pos < t_pos
-        weight = scores * jnp.exp(jnp.where(before, col_f + row_f, col_b + row_b))
+        before = before_of(d)
+        rows = rows_of_gate[j]
+        weight = scores * jnp.exp(jnp.where(before, col_f + rows[0:1], col_b + rows[1:2]))
+        weights[m] = weight
         diag = diag * jnp.exp(col_i)
         z_f = jnp.sum(jnp.where(before, weight, 0.0), axis=1, keepdims=True) + diag
         z_b = jnp.sum(jnp.where(before, 0.0, weight), axis=1, keepdims=True)
+        sums[m] = jnp.where(lane_z == 0, z_f, jnp.where(lane_z == 1, z_b, diag))
+    def weigh(k, _):
+        for j in range(2):
+            weigh_head((my_rank + 1 + k) % half, k, j)
+        return 0
+
+    lax.fori_loop(0, half, weigh, 0)
+    pass_until(2)
+    state_copy().wait_recv()
+
+    def segment_head(d, k, j):
+        m = 2 * k + j
+        start = pl.multiple_of(d * tok, tok)
+        col = cols[j, pl.ds(start, tok), :]
+        carried = jnp.exp(jnp.where(upper, col[:, 0:1], col[:, 1:2]))
+        qs = scaled(j, d) * carried
+        normal = state_in[j, dk:, 0:dk].astype(jnp.float32)
+        z_state = jnp.sum(qs * (normal[0:1] + normal[1:2]), axis=1, keepdims=True)
+        z = sums[m]
+        z_f, z_b, diag = z[:, 0:1], z[:, 1:2], z[:, 2:3]
+        z_f = z_f + jnp.where(upper, z_state, 0.0)
+        z_b = z_b + jnp.where(upper, 0.0, z_state)
         inv_f = 1.0 / jnp.maximum(jnp.abs(z_f), 1.0)
         inv_b = 1.0 / jnp.maximum(jnp.abs(z_b), 1.0)
-        probs = (weight * jnp.where(before, inv_f, inv_b)).astype(jnp.bfloat16)
+        probs = (weights[m] * jnp.where(before_of(d), inv_f, inv_b)).astype(jnp.bfloat16)
+        vall = recv[j, :, 0:tok, 2 * dk : 2 * dk + dv].reshape(length, dv)
         total = jnp.dot(probs, vall, preferred_element_type=jnp.float32)
-        total = total + (diag * inv_f) * recv[d, 0:tok, 2 * dk : 2 * dk + dv].astype(jnp.float32)
+        total = total + jnp.dot(
+            (qs * jnp.where(upper, inv_f, inv_b)).astype(jnp.bfloat16),
+            state_in[j, 0:dk],
+            preferred_element_type=jnp.float32,
+        )
+        total = total + (diag * inv_f) * recv[j, d, 0:tok, 2 * dk : 2 * dk + dv].astype(jnp.float32)
+        amp = params[j, n : n + 1, 0:dv]
         total = total * lax.rsqrt(jnp.mean(total * total, axis=1, keepdims=True) + EPS) * amp
-        mixed[d] = total.astype(jnp.bfloat16)
-
-        @pl.when(j >= 1)
-        def _():
-            mixed_copy(j, me).start()
-
-        @pl.when(j == 0)
-        def _():
-            for late in range(max(share - 1, 1), share):
-                pass_on(late)
-
-        @pl.when(j == n // 2)
-        def _():
-            for late in range(share, share + (PIECES - share) // 2):
-                pass_on(late)
+        mixed[j, d] = total.astype(jnp.bfloat16)
+
+    def segment(k, _):
+        d = (my_rank + 1 + k) % half
+        for j in range(2):
+            segment_head(d, k, j)
+
+        @pl.when(k < half - 1)
+        def _():
+            for j in range(2):
+                mixed_copy(k + 1, j, my_rank).start()
 
         return 0
 
-    lax.fori_loop(0, n, segment, 0)
-    for j in range(share + (PIECES - share) // 2, PIECES):
-        pass_on(j)
-    mrecv[me] = mixed[me]
+    lax.fori_loop(0, half, segment, 0)
+    pass_until(3)
+    for j in range(2):
+        mrecv[my_rank + j * half] = mixed[j, my_rank]
     sub_r = lax.broadcasted_iota(jnp.int32, (rows_in, tok), 0).astype(jnp.float32)
     at = sub_r + (my_z * rows_in).astype(jnp.float32)
 
@@ -350,8 +466,10 @@
 
     lax.fori_loop(0, nz, tables, 0)
     sig = jax.nn.sigmoid(logits_ref[0].astype(jnp.float32))
-    for o in range(1, n):
-        mixed_copy(o, (me + n - o) % n).wait_recv()
+    pass_until(4)
+    for o in range(1, half):
+        for j in range(2):
+            mixed_copy(o, j, (my_rank + half - o) % half).wait_recv()
     gated = jnp.concatenate([mrecv[h].astype(jnp.float32) for h in range(n)], axis=1) * sig
     gated = gated.astype(jnp.bfloat16)
     own_w.wait()
@@ -506,27 +624,29 @@
 
         lax.fori_loop(0, PARTS, piece, 0)
 
-    def partial_copy(z, p):
+    def partial_copy(z, f):
         to = jnp.where(z < my_z, below, above)
         slot = jnp.where((z > my_z) & (to == z), nz, z)
         return pltpu.make_async_remote_copy(
-            src_ref=partial_out.at[z, p],
-            dst_ref=partial_in.at[slot, p],
-            send_sem=part_send.at[z, p],
-            recv_sem=part_recv.at[slot, p],
+            src_ref=partial_out.at[z, f],
+            dst_ref=partial_in.at[slot, f],
+            send_sem=part_send.at[z, f],
+            recv_sem=part_recv.at[slot, f],
             device_id=device(to, my_q),
             device_id_type=MESH,
         )
 
-    def partial_arrive(slot, p):
+    def partial_arrive(slot, f):
         pltpu.make_async_remote_copy(
-            src_ref=partial_out.at[0, p],
-            dst_ref=partial_in.at[slot, p],
-            send_sem=part_send.at[0, p],
-            recv_sem=part_recv.at[slot, p],
+            src_ref=partial_out.at[0, f],
+            dst_ref=partial_in.at[slot, f],
+            send_sem=part_send.at[0, f],
+            recv_sem=part_recv.at[slot, f],
             device_id=device(above, my_q),
             device_id_type=MESH,
         ).wait_recv()
+
+    fine = part // SUBS
 
     def combine(z, p):
         plane_all(*back_way, z, p).wait_recv()
@@ -534,21 +654,29 @@
         mine = jnp.dot(table_hi[z], block, preferred_element_type=jnp.float32) + jnp.dot(
             table_lo[z], block, preferred_element_type=jnp.float32
         )
-        total[PARTS] = mine
 
         @pl.when(z == my_z)
         def _():
-            total[p] += total[PARTS]
-
-        @pl.when(z != my_z)
-        def _():
-            @pl.when(~edge)
-            def _():
-                partial_arrive(z, p)
-                total[PARTS] += partial_in[z, p].astype(jnp.float32)
-
-            partial_out[z, p] = total[PARTS].astype(jnp.bfloat16)
-            partial_copy(z, p).start()
+            total[p] += mine
+
+        @pl.when((z != my_z) & edge)
+        def _():
+            for i in range(SUBS):
+                f = p * SUBS + i
+                partial_out[z, f] = mine[:, i * fine : (i + 1) * fine].astype(jnp.bfloat16)
+                partial_copy(z, f).start()
+
+        @pl.when((z != my_z) & ~edge)
+        def _():
+            total[PARTS] = mine
+            for i in range(SUBS):
+                f = p * SUBS + i
+                partial_arrive(z, f)
+                partial_out[z, f] = (
+                    total[PARTS, :, i * fine : (i + 1) * fine]
+                    + partial_in[z, f].astype(jnp.float32)
+                ).astype(jnp.bfloat16)
+                partial_copy(z, f).start()
 
     def combine_all(k):
         def one(p, _):
@@ -558,12 +686,12 @@
         lax.fori_loop(0, PARTS, one, 0)
 
     dispatch(0, 0, PARTS)
-    half = PARTS // 2
+    midway = PARTS // 2
 
     def tick(k, _):
         last = k == nz - 1
         stop = jnp.where(last, 0, PARTS)
-        early = jnp.minimum(jnp.where(k == 0, half, jnp.where(edge, jnp.where(k == 1, half // 2, half), PARTS)), stop)
+        early = jnp.minimum(jnp.where(k == 0, midway, jnp.where(edge, jnp.where(k == 1, midway // 2, midway), PARTS)), stop)
         dispatch(k + 1, 0, early)
 
         @pl.when(~edge & (k == nz - 2))
@@ -592,27 +720,34 @@
         send_back(0)
         if nz > 2:
             combine_all(1)
-        late = max(nz - 2, 1)
-
-        def one(m, _):
-            combine(by_distance(nz - 1 - m % late), m // late)
+
+        def one(s, _):
+            for behind in range(nz - 2):
+                p = s - behind
+
+                @pl.when((p >= 0) & (p < PARTS))
+                def _():
+                    combine(by_distance(nz - 1 - behind), p)
+
             return 0
 
-        lax.fori_loop(0, (nz - 2) * PARTS, one, 0)
+        lax.fori_loop(0, PARTS + max(nz - 3, 0), one, 0)
 
     combine_all(0)
-    for p in range(PARTS):
+    for f in range(PARTS * SUBS):
+        p, at = f // SUBS, pl.ds(f % SUBS * fine, fine)
+
         @pl.when(has_above)
         def _():
-            partial_arrive(my_z, p)
-            total[p] += partial_in[my_z, p].astype(jnp.float32)
+            partial_arrive(my_z, f)
+            total[p, :, at] += partial_in[my_z, f].astype(jnp.float32)
 
         @pl.when(has_below)
         def _():
-            partial_arrive(nz, p)
-            total[p] += partial_in[nz, p].astype(jnp.float32)
-
-        out_ref[0, :, p * part : (p + 1) * part] = total[p].astype(jnp.bfloat16)
+            partial_arrive(nz, f)
+            total[p, :, at] += partial_in[nz, f].astype(jnp.float32)
+
+        out_ref[0, :, f * fine : (f + 1) * fine] = total[p, :, at].astype(jnp.bfloat16)
 
     def drain(i, _):
         z, p = i // PARTS, i % PARTS
@@ -629,24 +764,30 @@
 
         @pl.when(z != my_z)
         def _():
-            partial_copy(z, p).wait_send()
+            for i in range(SUBS):
+                partial_copy(z, p * SUBS + i).wait_send()
 
         return 0
 
     lax.fori_loop(0, nz * PARTS, drain, 0)
     for o in range(1, nz):
         meta_copy((my_z + o) % nz, my_z).wait_send()
-    for o in range(1, n):
-        qkv_copy(o).wait_send()
-        mixed_copy(o, me).wait_send()
+    for o in range(1, half):
+        for j in range(2):
+            qkv_copy(o, j).wait_send()
+            mixed_copy(o, j, my_rank).wait_send()
+    param_copy(my_half).wait_send()
+    state_copy().wait_send()
     own_copy().wait_send()
     for o in range(1, chips):
         for p in range(PIECES):
             wc_copy(o, p).wait_send()
-        for j in range(share):
-            wx_copy(o, first_piece + j).wait_send()
+        for j in range(direct):
+            p = (first_piece + j) % PIECES
+            wx_copy(o, p).wait_send()
             for yo in range(1, ny):
-                wy_copy(o, first_piece + j, yo).wait_send()
+                if onward(j, yo):
+                    wy_copy(o, p, yo).wait_send()
 
 
 def on_device(
@@ -672,7 +813,8 @@
     n, dpn = lax.axis_size("sp"), lax.axis_size("dp")
     tok, width = residual_input.shape[1:]
     dk, dv = queries.shape[2] // n, values.shape[2] // n
-    length, devices, ff = n * tok, n * dpn, gate_weight.shape[2]
+    half = n // 2
+    length, devices, ff = half * tok, n * dpn, gate_weight.shape[2]
     cap, chips = 4 * tok // devices, dpn // 2
     ny = chips if n % chips == 0 else 1
     nz, plane = n // ny, ny * dpn
@@ -696,10 +838,16 @@
         scratch_shapes=[pltpu.VMEM(x.shape, x.dtype) for x in operands]
         + [
             pltpu.VMEM((n, tok + GATE_ROWS, 2 * dk + dv), bf16),
-            pltpu.VMEM((n, tok + GATE_ROWS, 2 * dk + dv), bf16),
+            pltpu.VMEM((2, half, tok + GATE_ROWS, 2 * dk + dv), bf16),
             pltpu.VMEM((128, tok), f32),
-            pltpu.VMEM((length, 128), f32),
-            pltpu.VMEM((n, tok, dv), bf16),
+            pltpu.VMEM((2, -(-(n + 2) // 8) * 8, max(tok, dv)), f32),
+            pltpu.VMEM((2, 8, length), f32),
+            pltpu.VMEM((2, length, 128), f32),
+            pltpu.VMEM((n, tok, length), f32),
+            pltpu.VMEM((n, tok, 128), f32),
+            pltpu.VMEM((2, dk + GATE_ROWS, dv), bf16),
+            pltpu.VMEM((2, dk + GATE_ROWS, dv), bf16),
+            pltpu.VMEM((2, half, tok, dv), bf16),
             pltpu.VMEM((n, tok, dv), bf16),
             pltpu.VMEM((dpn,) + output_projection.shape, bf16),
             pltpu.VMEM((tok, width), f32),
@@ -713,18 +861,19 @@
             pltpu.VMEM((rows_in, ff), bf16),
             pltpu.VMEM((nz, PARTS, plane, cap, part), bf16),
             pltpu.VMEM((nz, PARTS, plane, cap, part), bf16),
-            pltpu.VMEM((nz, PARTS, tok, part), bf16),
-            pltpu.VMEM((nz + 1, PARTS, tok, part), bf16),
+            pltpu.VMEM((nz, PARTS * SUBS, tok, part // SUBS), bf16),
+            pltpu.VMEM((nz + 1, PARTS * SUBS, tok, part // SUBS), bf16),
             pltpu.VMEM((PARTS + 1, tok, part), f32),
             dma((len(operands),)),
-            dma((n,)), dma((n,)), dma((n,)), dma((n,)),
+            dma((half, 2)), dma((half, 2)), dma(()), dma(()), dma(()), dma(()),
+            dma((half, 2)), dma((half, 2)),
             dma((chips, PIECES)), dma((chips, PIECES)), dma((chips, PIECES, ny)),
             dma((chips, PIECES)), dma((chips, PIECES)),
             dma(()),
             dma((nz,)), dma((nz,)),
             dma((nz, PARTS)), dma((nz, PARTS)), dma((nz, PARTS)),
             dma((nz, PARTS)), dma((nz, PARTS)), dma((nz, PARTS)), dma((nz, PARTS)),
-            dma((nz, PARTS)), dma((nz + 1, PARTS)),
+            dma((nz, PARTS * SUBS)), dma((nz + 1, PARTS * SUBS)),
         ],
         compiler_params=pltpu.CompilerParams(
             collective_id=0, has_side_effects=True, vmem_limit_bytes=60 * 1024 * 1024

time: 114 us -> 107 us (0.939)
  Pallas kernels: 113 us -> 106 us
    pallas_call x1, Pallas kernels: 113 us -> 106 us  [on_device(): pl.pallas_call(partial(layer_kernel, n=n, dpn=dpn, inputs=len(operands)),...]
where the time goes in v3:
time: 107 us
  Pallas kernels  106 us (99%)
    pallas_call x1, Pallas kernels, on_device(): pl.pallas_call(partial(layer_kernel, n=n, dpn=dpn, inputs=len(operands)),...  106 us

profile of v3, /device:TPU:0, one launch (start us, length us, event | category | flops | bytes accessed | tf_op | source)
XLA Modules:
  0.0 106.9 jit_solution(8569284752628493739)
XLA Ops:
  0.0 106.1 %shard_map.172 = bf16[1,128,2048]{2,1,0:T(8,128)(2,1)S(1)} custom-call(bf16[1,128,512]{2,1,0:T(8,128)(2,1)} %refs_0_.1, bf16[1,128,512]{2,1,0:T(8,128)(2,1)} %refs_1_.1, bf16[1,128,1024]{2,1,0:T(8,128)(2,1)} %refs_2_.1, bf16[1,32,128]{2,1,0:T(8,128)(2,1)} %bitcast.7, f32[1,2]{1,0:T(1,128)} %refs_4_.1, f32[1,1,1024]{2,1,0:T(1,128)} %refs_5_.1, ...), custom_call_target="tpu_custom_call" | custom-call | tf_op jit(solution)/shard_map/pallas_call | solution.py:833
  106.1 0.8 copy.20

commit v4 on v3

--- a/solution.py
+++ b/solution.py
@@ -33,7 +33,7 @@
         send, recv, gates_t, params, rows_of_gate, cols, weights, sums, state_out, state_in,
         mixed, mrecv, wfull, proj,
         meta, table_t, table_hi, table_lo, line, outgoing, incoming, hs, produced, returned,
-        partial_out, partial_in, total,
+        partial_out, partial_in, total, partial,
         in_sem, send_sem, recv_sem, param_send, param_recv, state_send, state_recv, msend_sem, mrecv_sem, wx_send, wx_recv, wy_send, wc_send,
         wc_recv, wl_sem, meta_send, meta_recv, up_send, down_send, line_recv,
         out_send, out_recv, back_send, back_recv, part_send, part_recv,
@@ -106,25 +106,28 @@
         if i not in early:
             loads[i].start()
 
+    def all_of(ref, send_sem, recv_sem):
+        return pltpu.make_async_remote_copy(
+            src_ref=ref,
+            dst_ref=ref,
+            send_sem=send_sem,
+            recv_sem=recv_sem,
+            device_id={"sp": opposite, "dp": my_dp},
+            device_id_type=MESH,
+        )
+
     def qkv_copy(o, j):
         return pltpu.make_async_remote_copy(
             src_ref=send.at[(my_rank + o) % half + j * half],
             dst_ref=recv.at[j, my_rank],
-            send_sem=send_sem.at[o, j],
-            recv_sem=recv_sem.at[o, j],
+            send_sem=send_sem,
+            recv_sem=recv_sem,
             device_id={"sp": first + (my_rank + o) % half, "dp": my_dp},
             device_id_type=MESH,
         )
 
-    def qkv_arrival(o, j):
-        return pltpu.make_async_remote_copy(
-            src_ref=send.at[(my_rank + o) % half + j * half],
-            dst_ref=recv.at[j, (my_rank + half - o) % half],
-            send_sem=send_sem.at[o, j],
-            recv_sem=recv_sem.at[o, j],
-            device_id={"sp": first + (my_rank + o) % half, "dp": my_dp},
-            device_id_type=MESH,
-        )
+    def qkv_all():
+        return all_of(send.at[pl.ds(0, 2 * (half - 1))], send_sem, recv_sem)
 
     def param_copy(slot):
         return pltpu.make_async_remote_copy(
@@ -159,8 +162,8 @@
         return pltpu.make_async_remote_copy(
             src_ref=w_ref.at[rows_of(p)],
             dst_ref=wfull.at[my_dp, rows_of(p)],
-            send_sem=wx_send.at[o, p],
-            recv_sem=wx_recv.at[o, p],
+            send_sem=wx_send.at[o - 1],
+            recv_sem=wx_recv.at[o - 1, p],
             device_id={"sp": me, "dp": ((my_x + o) % chips) * 2 + my_core},
             device_id_type=MESH,
         )
@@ -172,8 +175,8 @@
         return pltpu.make_async_remote_copy(
             src_ref=wfull.at[from_chip(o), rows_of(p)],
             dst_ref=wfull.at[from_chip(o), rows_of(p)],
-            send_sem=wy_send.at[o, p, yo],
-            recv_sem=wx_recv.at[o, p],
+            send_sem=wy_send.at[o - 1, yo - 1],
+            recv_sem=wx_recv.at[o - 1, p],
             device_id={"sp": my_z * ny + (my_y + yo) % ny, "dp": my_dp},
             device_id_type=MESH,
         )
@@ -182,8 +185,8 @@
         return pltpu.make_async_remote_copy(
             src_ref=wfull.at[from_chip(o), rows_of(p)],
             dst_ref=wfull.at[from_chip(o), rows_of(p)],
-            send_sem=wc_send.at[o, p],
-            recv_sem=wc_recv.at[o, p],
+            send_sem=wc_send.at[o],
+            recv_sem=wc_recv.at[o],
             device_id={"sp": me, "dp": my_x * 2 + 1 - my_core},
             device_id_type=MESH,
         )
@@ -192,8 +195,8 @@
         return pltpu.make_async_remote_copy(
             src_ref=w_ref,
             dst_ref=wfull.at[my_dp],
-            send_sem=wc_send.at[0, 0],
-            recv_sem=wc_recv.at[0, 0],
+            send_sem=wc_send.at[0],
+            recv_sem=wc_recv.at[0],
             device_id={"sp": me, "dp": my_x * 2 + 1 - my_core},
             device_id_type=MESH,
         )
@@ -272,8 +275,8 @@
         return pltpu.make_async_remote_copy(
             src_ref=meta.at[my_z],
             dst_ref=meta.at[slot],
-            send_sem=meta_send.at[z],
-            recv_sem=meta_recv.at[slot],
+            send_sem=meta_send,
+            recv_sem=meta_recv,
             device_id=device(z, my_q),
             device_id_type=MESH,
         )
@@ -281,16 +284,15 @@
     for o in range(1, nz):
         meta_copy((my_z + o) % nz, my_z).start()
 
-    stops = [PIECES * i // 8 for i in (2, 3, 5, 6, 8)]
+    stops = [PIECES * i // 8 for i in (2, 3, 4, 8, 8)]
 
     def pass_until(i):
         for j in range(stops[i - 1] if i else 0, stops[i]):
             pass_on(j)
 
     pass_until(0)
-    for o in range(1, half):
-        for j in range(2):
-            qkv_arrival(o, j).wait_recv()
+    if half > 1:
+        qkv_all().wait_recv()
     param_copy(1 - my_half).wait_recv()
 
     upper = my_half == 1
@@ -357,11 +359,14 @@
         return pltpu.make_async_remote_copy(
             src_ref=mixed.at[j, (my_rank + o) % half],
             dst_ref=mrecv.at[rank + j * half],
-            send_sem=msend_sem.at[o, j],
-            recv_sem=mrecv_sem.at[o, j],
+            send_sem=msend_sem,
+            recv_sem=mrecv_sem,
             device_id={"sp": first + (my_rank + o) % half, "dp": my_dp},
             device_id_type=MESH,
         )
+
+    def mixed_all():
+        return all_of(mrecv.at[pl.ds(0, 2 * (half - 1))], msend_sem, mrecv_sem)
 
     def scaled(j, d):
         return recv[j, d, 0:tok, dk : 2 * dk].astype(jnp.float32) * scale
@@ -451,10 +456,6 @@
     def tables(o, _):
         z = (my_z + o) % nz
 
-        @pl.when(o > 0)
-        def _():
-            meta_copy(z, z).wait_recv()
-
         rows = meta[z]
         hit_0, hit_1 = at == rows[0:1], at == rows[1:2]
         table_t[z] = (jnp.where(hit_0, 1.0, 0.0) + jnp.where(hit_1, 1.0, 0.0)).astype(jnp.bfloat16)
@@ -464,19 +465,18 @@
         table_lo[z] = (weighted - high.astype(jnp.float32)).astype(jnp.bfloat16)
         return 0
 
+    if nz > 1:
+        all_of(meta.at[pl.ds(0, nz - 1)], meta_send, meta_recv).wait_recv()
     lax.fori_loop(0, nz, tables, 0)
     sig = jax.nn.sigmoid(logits_ref[0].astype(jnp.float32))
     pass_until(4)
-    for o in range(1, half):
-        for j in range(2):
-            mixed_copy(o, j, (my_rank + half - o) % half).wait_recv()
+    if half > 1:
+        mixed_all().wait_recv()
     gated = jnp.concatenate([mrecv[h].astype(jnp.float32) for h in range(n)], axis=1) * sig
     gated = gated.astype(jnp.bfloat16)
     own_w.wait()
-    own_copy().wait_recv()
-    for p in range(PIECES):
-        for o in range(1, chips):
-            wc_copy(o, p).wait_recv()
+    for o in range(chips):
+        all_of(w_ref, wc_send.at[o], wc_recv.at[o]).wait_recv()
     for j in range(dpn):
         proj[:, j * wcol : (j + 1) * wcol] = jnp.dot(
             gated, wfull[j], preferred_element_type=jnp.float32
@@ -497,7 +497,7 @@
         return pltpu.make_async_remote_copy(
             src_ref=line.at[z, p],
             dst_ref=line.at[z, p],
-            send_sem=sems.at[z, p],
+            send_sem=sems.at[z],
             recv_sem=line_recv.at[z, p],
             device_id=device(to, my_q),
             device_id_type=MESH,
@@ -538,7 +538,7 @@
         return pltpu.make_async_remote_copy(
             src_ref=src.at[z, p, q_src],
             dst_ref=dst.at[z, p, q_dst],
-            send_sem=sems[0].at[z, p],
+            send_sem=sems[0],
             recv_sem=sems[1].at[z, p],
             device_id=device(my_z, q_to),
             device_id_type=MESH,
@@ -558,7 +558,7 @@
         return pltpu.make_async_remote_copy(
             src_ref=src.at[z, p, others],
             dst_ref=dst.at[z, p, others],
-            send_sem=sems[0].at[z, p],
+            send_sem=sems[0],
             recv_sem=sems[1].at[z, p],
             device_id=device(my_z, (my_q + 1) % plane),
             device_id_type=MESH,
@@ -590,18 +590,32 @@
             plane_all(*out_way, z, p).wait_recv()
             return 0
 
-        lax.fori_loop(0, PARTS, arrive, 0)
+        split = max(PARTS // 2, 1)
+
+        def sides(first, last, at):
+            x = jnp.concatenate(
+                [incoming[z, p].reshape(rows_in, part) for p in range(first, last)], axis=1
+            )
+            rows = slice(first * part, last * part)
+            a = jnp.dot(x, gate_ref[0, rows, at], preferred_element_type=jnp.float32)
+            u = jnp.dot(x, up_ref[0, rows, at], preferred_element_type=jnp.float32)
+            return a, u
+
+        def begin_tile(t, _):
+            at = pl.ds(pl.multiple_of(t * FF_TILE, FF_TILE), FF_TILE)
+            partial[0, :, at], partial[1, :, at] = sides(0, split, at)
+            return 0
 
         def up_tile(t, _):
             at = pl.ds(pl.multiple_of(t * FF_TILE, FF_TILE), FF_TILE)
-            x = jnp.concatenate(
-                [incoming[z, p].reshape(rows_in, part) for p in range(PARTS)], axis=1
-            )
-            a = jnp.dot(x, gate_ref[0, :, at], preferred_element_type=jnp.float32)
-            u = jnp.dot(x, up_ref[0, :, at], preferred_element_type=jnp.float32)
+            a, u = sides(split, PARTS, at)
+            a, u = a + partial[0, :, at], u + partial[1, :, at]
             hs[:, at] = (jax.nn.silu(a) * u).astype(jnp.bfloat16)
             return 0
 
+        lax.fori_loop(0, split, arrive, 0)
+        lax.fori_loop(0, ff // FF_TILE, begin_tile, 0)
+        lax.fori_loop(split, PARTS, arrive, 0)
         lax.fori_loop(0, ff // FF_TILE, up_tile, 0)
 
         def down_tile(p, _):
@@ -630,7 +644,7 @@
         return pltpu.make_async_remote_copy(
             src_ref=partial_out.at[z, f],
             dst_ref=partial_in.at[slot, f],
-            send_sem=part_send.at[z, f],
+            send_sem=part_send,
             recv_sem=part_recv.at[slot, f],
             device_id=device(to, my_q),
             device_id_type=MESH,
@@ -640,7 +654,7 @@
         pltpu.make_async_remote_copy(
             src_ref=partial_out.at[0, f],
             dst_ref=partial_in.at[slot, f],
-            send_sem=part_send.at[0, f],
+            send_sem=part_send,
             recv_sem=part_recv.at[slot, f],
             device_id=device(above, my_q),
             device_id_type=MESH,
@@ -749,45 +763,37 @@
 
         out_ref[0, :, f * fine : (f + 1) * fine] = total[p, :, at].astype(jnp.bfloat16)
 
-    def drain(i, _):
-        z, p = i // PARTS, i % PARTS
-        plane_all(*out_way, z, p).wait_send()
-        plane_all(*back_way, z, p).wait_send()
-
+    def drain(z, _):
         @pl.when((z <= my_z) & has_above)
         def _():
-            line_copy(z, p, above, up_send).wait_send()
+            all_of(line.at[z], up_send.at[z], meta_recv).wait_send()
 
         @pl.when((z >= my_z) & has_below)
         def _():
-            line_copy(z, p, below, down_send).wait_send()
-
-        @pl.when(z != my_z)
-        def _():
-            for i in range(SUBS):
-                partial_copy(z, p * SUBS + i).wait_send()
+            all_of(line.at[z], down_send.at[z], meta_recv).wait_send()
 
         return 0
 
-    lax.fori_loop(0, nz * PARTS, drain, 0)
-    for o in range(1, nz):
-        meta_copy((my_z + o) % nz, my_z).wait_send()
-    for o in range(1, half):
-        for j in range(2):
-            qkv_copy(o, j).wait_send()
-            mixed_copy(o, j, my_rank).wait_send()
+    lax.fori_loop(0, nz, drain, 0)
+    if nz > 1:
+        all_of(meta.at[pl.ds(0, nz - 1)], meta_send, meta_recv).wait_send()
+        all_of(partial_out.at[pl.ds(0, nz - 1)], part_send, meta_recv).wait_send()
+    others = pl.ds(0, plane - 1)
+    all_of(outgoing.at[:, :, others], out_send, meta_recv).wait_send()
+    all_of(produced.at[:, :, others], back_send, meta_recv).wait_send()
+    if half > 1:
+        qkv_all().wait_send()
+        mixed_all().wait_send()
     param_copy(my_half).wait_send()
     state_copy().wait_send()
-    own_copy().wait_send()
+    for o in range(chips):
+        all_of(w_ref, wc_send.at[o], wc_recv.at[o]).wait_send()
     for o in range(1, chips):
-        for p in range(PIECES):
-            wc_copy(o, p).wait_send()
-        for j in range(direct):
-            p = (first_piece + j) % PIECES
-            wx_copy(o, p).wait_send()
-            for yo in range(1, ny):
-                if onward(j, yo):
-                    wy_copy(o, p, yo).wait_send()
+        held = w_ref.at[pl.ds(0, direct * piece)]
+        all_of(held, wx_send.at[o - 1], wc_recv.at[0]).wait_send()
+        for yo in range(1, ny):
+            held = w_ref.at[pl.ds(0, sum(onward(j, yo) for j in range(share)) * piece)]
+            all_of(held, wy_send.at[o - 1, yo - 1], wc_recv.at[0]).wait_send()
 
 
 def on_device(
@@ -864,16 +870,15 @@
             pltpu.VMEM((nz, PARTS * SUBS, tok, part // SUBS), bf16),
             pltpu.VMEM((nz + 1, PARTS * SUBS, tok, part // SUBS), bf16),
             pltpu.VMEM((PARTS + 1, tok, part), f32),
+            pltpu.VMEM((2, rows_in, ff), f32),
             dma((len(operands),)),
-            dma((half, 2)), dma((half, 2)), dma(()), dma(()), dma(()), dma(()),
-            dma((half, 2)), dma((half, 2)),
-            dma((chips, PIECES)), dma((chips, PIECES)), dma((chips, PIECES, ny)),
-            dma((chips, PIECES)), dma((chips, PIECES)),
-            dma(()),
-            dma((nz,)), dma((nz,)),
-            dma((nz, PARTS)), dma((nz, PARTS)), dma((nz, PARTS)),
-            dma((nz, PARTS)), dma((nz, PARTS)), dma((nz, PARTS)), dma((nz, PARTS)),
-            dma((nz, PARTS * SUBS)), dma((nz + 1, PARTS * SUBS)),
+            dma(()), dma(()), dma(()), dma(()), dma(()), dma(()), dma(()), dma(()),
+            dma((max(chips - 1, 1),)), dma((max(chips - 1, 1), PIECES)),
+            dma((max(chips - 1, 1), max(ny - 1, 1))), dma((chips,)), dma((chips,)),
+            dma(()), dma(()), dma(()),
+            dma((nz,)), dma((nz,)), dma((nz, PARTS)),
+            dma(()), dma((nz, PARTS)), dma(()), dma((nz, PARTS)),
+            dma(()), dma((nz + 1, PARTS * SUBS)),
         ],
         compiler_params=pltpu.CompilerParams(
             collective_id=0, has_side_effects=True, vmem_limit_bytes=60 * 1024 * 1024

time: 107 us -> 101 us (0.944)
  Pallas kernels: 106 us -> 101 us
    pallas_call x1, Pallas kernels: 106 us -> 101 us  [on_device(): pl.pallas_call(partial(layer_kernel, n=n, dpn=dpn, inputs=len(operands)),...]
where the time goes in v4:
time: 101 us
  Pallas kernels  101 us (100%)
    pallas_call x1, Pallas kernels, on_device(): pl.pallas_call(partial(layer_kernel, n=n, dpn=dpn, inputs=len(operands)),...  101 us

profile of v4, /device:TPU:0, one launch (start us, length us, event | category | flops | bytes accessed | tf_op | source)
XLA Modules:
  0.0 101.3 jit_solution(3522877547721940672)
XLA Ops:
  0.0 100.5 %shard_map.172 = bf16[1,128,2048]{2,1,0:T(8,128)(2,1)S(1)} custom-call(bf16[1,128,512]{2,1,0:T(8,128)(2,1)} %refs_0_.1, bf16[1,128,512]{2,1,0:T(8,128)(2,1)} %refs_1_.1, bf16[1,128,1024]{2,1,0:T(8,128)(2,1)} %refs_2_.1, bf16[1,32,128]{2,1,0:T(8,128)(2,1)} %bitcast.7, f32[1,2]{1,0:T(1,128)} %refs_4_.1, f32[1,1,1024]{2,1,0:T(1,128)} %refs_5_.1, ...), custom_call_target="tpu_custom_call" | custom-call | tf_op jit(solution)/shard_map/pallas_call | solution.py:839
  100.5 0.8 copy.20

commit v5 on v4

--- a/solution.py
+++ b/solution.py
@@ -39,7 +39,7 @@
         out_send, out_recv, back_send, back_recv, part_send, part_recv,
     ) = rest
     loads = [pltpu.make_async_copy(hbm[i], local[i], in_sem.at[i]) for i in range(inputs)]
-    early = (0, 1, 2, 3, 8)
+    early = (0, 1, 2, 3, 4, 5, 6, 8)
     for i in early:
         loads[i].start()
     tok = q_ref.shape[1]
@@ -101,131 +101,7 @@
             (GATE_ROWS, send.shape[2] - tok), jnp.bfloat16
         )
 
-    pl.semaphore_wait(barrier, n - 1 + plane - 1)
-    for i in range(inputs):
-        if i not in early:
-            loads[i].start()
-
-    def all_of(ref, send_sem, recv_sem):
-        return pltpu.make_async_remote_copy(
-            src_ref=ref,
-            dst_ref=ref,
-            send_sem=send_sem,
-            recv_sem=recv_sem,
-            device_id={"sp": opposite, "dp": my_dp},
-            device_id_type=MESH,
-        )
-
-    def qkv_copy(o, j):
-        return pltpu.make_async_remote_copy(
-            src_ref=send.at[(my_rank + o) % half + j * half],
-            dst_ref=recv.at[j, my_rank],
-            send_sem=send_sem,
-            recv_sem=recv_sem,
-            device_id={"sp": first + (my_rank + o) % half, "dp": my_dp},
-            device_id_type=MESH,
-        )
-
-    def qkv_all():
-        return all_of(send.at[pl.ds(0, 2 * (half - 1))], send_sem, recv_sem)
-
-    def param_copy(slot):
-        return pltpu.make_async_remote_copy(
-            src_ref=params.at[my_half],
-            dst_ref=params.at[slot],
-            send_sem=param_send,
-            recv_sem=param_recv,
-            device_id={"sp": opposite, "dp": my_dp},
-            device_id_type=MESH,
-        )
-
-    def state_copy():
-        return pltpu.make_async_remote_copy(
-            src_ref=state_out,
-            dst_ref=state_in,
-            send_sem=state_send,
-            recv_sem=state_recv,
-            device_id={"sp": opposite, "dp": my_dp},
-            device_id_type=MESH,
-        )
-
-    piece = w_ref.shape[0] // PIECES
-
-    share = PIECES // ny
-    direct = share + (EXTRA if ny > 1 else 0)
-    first_piece = my_y * share
-
-    def rows_of(p):
-        return pl.ds(pl.multiple_of(p * piece, piece), piece)
-
-    def wx_copy(o, p):
-        return pltpu.make_async_remote_copy(
-            src_ref=w_ref.at[rows_of(p)],
-            dst_ref=wfull.at[my_dp, rows_of(p)],
-            send_sem=wx_send.at[o - 1],
-            recv_sem=wx_recv.at[o - 1, p],
-            device_id={"sp": me, "dp": ((my_x + o) % chips) * 2 + my_core},
-            device_id_type=MESH,
-        )
-
-    def from_chip(o):
-        return ((my_x + chips - o) % chips) * 2 + my_core
-
-    def wy_copy(o, p, yo):
-        return pltpu.make_async_remote_copy(
-            src_ref=wfull.at[from_chip(o), rows_of(p)],
-            dst_ref=wfull.at[from_chip(o), rows_of(p)],
-            send_sem=wy_send.at[o - 1, yo - 1],
-            recv_sem=wx_recv.at[o - 1, p],
-            device_id={"sp": my_z * ny + (my_y + yo) % ny, "dp": my_dp},
-            device_id_type=MESH,
-        )
-
-    def wc_copy(o, p):
-        return pltpu.make_async_remote_copy(
-            src_ref=wfull.at[from_chip(o), rows_of(p)],
-            dst_ref=wfull.at[from_chip(o), rows_of(p)],
-            send_sem=wc_send.at[o],
-            recv_sem=wc_recv.at[o],
-            device_id={"sp": me, "dp": my_x * 2 + 1 - my_core},
-            device_id_type=MESH,
-        )
-
-    def own_copy():
-        return pltpu.make_async_remote_copy(
-            src_ref=w_ref,
-            dst_ref=wfull.at[my_dp],
-            send_sem=wc_send.at[0],
-            recv_sem=wc_recv.at[0],
-            device_id={"sp": me, "dp": my_x * 2 + 1 - my_core},
-            device_id_type=MESH,
-        )
-
-    def onward(j, yo):
-        return j < share and (j >= EXTRA or yo < ny - 1)
-
-    def pass_on(j):
-        p = (first_piece + j) % PIECES
-        for o in range(1, chips):
-            wx_copy(o, p).wait_recv()
-            wc_copy(o, p).start()
-            for yo in range(1, ny):
-                if onward(j, yo):
-                    wy_copy(o, p, yo).start()
-
-    for o in range(1, half):
-        for j in range(2):
-            qkv_copy(o, j).start()
-    loads[8].wait()
-    for j in range(direct):
-        for o in range(1, chips):
-            wx_copy(o, (first_piece + j) % PIECES).start()
-    own_copy().start()
-    own_w = pltpu.make_async_copy(w_ref, wfull.at[my_dp], wl_sem)
-    own_w.start()
-    for j in range(2):
-        recv[j, my_rank] = send[my_rank + j * half]
-    for i in (4, 5, 6, 7, 9, 10, 11, 12, 13, 14):
+    for i in (4, 5, 6):
         loads[i].wait()
     for d in range(n):
         params[my_half, d : d + 1, 0:tok] = extra_ref[0, :, d * tok : (d + 1) * tok]
@@ -234,7 +110,140 @@
     params[my_half, n + 1 : n + 2] = jnp.where(
         lane_p == 0, offset_ref[0:1, 0:1], offset_ref[0:1, 1:2]
     )
+
+    pl.semaphore_wait(barrier, n - 1 + plane - 1)
+    for i in range(inputs):
+        if i not in early:
+            loads[i].start()
+
+    def all_of(ref, send_sem, recv_sem):
+        return pltpu.make_async_remote_copy(
+            src_ref=ref,
+            dst_ref=ref,
+            send_sem=send_sem,
+            recv_sem=recv_sem,
+            device_id={"sp": opposite, "dp": my_dp},
+            device_id_type=MESH,
+        )
+
+    def qkv_copy(o, j):
+        return pltpu.make_async_remote_copy(
+            src_ref=send.at[(my_rank + o) % half + j * half],
+            dst_ref=recv.at[j, my_rank],
+            send_sem=send_sem,
+            recv_sem=recv_sem,
+            device_id={"sp": first + (my_rank + o) % half, "dp": my_dp},
+            device_id_type=MESH,
+        )
+
+    def qkv_all():
+        return all_of(send.at[pl.ds(0, 2 * (half - 1))], send_sem, recv_sem)
+
+    def param_copy(slot):
+        return pltpu.make_async_remote_copy(
+            src_ref=params.at[my_half],
+            dst_ref=params.at[slot],
+            send_sem=param_send,
+            recv_sem=param_recv,
+            device_id={"sp": opposite, "dp": my_dp},
+            device_id_type=MESH,
+        )
+
+    def state_copy():
+        return pltpu.make_async_remote_copy(
+            src_ref=state_out,
+            dst_ref=state_in,
+            send_sem=state_send,
+            recv_sem=state_recv,
+            device_id={"sp": opposite, "dp": my_dp},
+            device_id_type=MESH,
+        )
+
+    piece = w_ref.shape[0] // PIECES
+
+    share = PIECES // ny
+    first_piece = my_y * share
+
+    def rows_of(p):
+        return pl.ds(pl.multiple_of(p * piece, piece), piece)
+
+    def wx_copy(o, p):
+        return pltpu.make_async_remote_copy(
+            src_ref=w_ref.at[rows_of(p)],
+            dst_ref=wfull.at[my_dp, rows_of(p)],
+            send_sem=wx_send.at[o - 1],
+            recv_sem=wx_recv.at[o - 1, p],
+            device_id={"sp": me, "dp": ((my_x + o) % chips) * 2 + my_core},
+            device_id_type=MESH,
+        )
+
+    def from_chip(o):
+        return ((my_x + chips - o) % chips) * 2 + my_core
+
+    def wy_copy(o, p, yo):
+        return pltpu.make_async_remote_copy(
+            src_ref=wfull.at[from_chip(o), rows_of(p)],
+            dst_ref=wfull.at[from_chip(o), rows_of(p)],
+            send_sem=wy_send.at[o - 1, yo - 1],
+            recv_sem=wx_recv.at[o - 1, p],
+            device_id={"sp": my_z * ny + (my_y + yo) % ny, "dp": my_dp},
+            device_id_type=MESH,
+        )
+
+    def wc_copy(o, p):
+        return pltpu.make_async_remote_copy(
+            src_ref=wfull.at[from_chip(o), rows_of(p)],
+            dst_ref=wfull.at[from_chip(o), rows_of(p)],
+            send_sem=wc_send.at[o],
+            recv_sem=wc_recv.at[o],
+            device_id={"sp": me, "dp": my_x * 2 + 1 - my_core},
+            device_id_type=MESH,
+        )
+
+    def own_copy():
+        return pltpu.make_async_remote_copy(
+            src_ref=w_ref,
+            dst_ref=wfull.at[my_dp],
+            send_sem=wc_send.at[0],
+            recv_sem=wc_recv.at[0],
+            device_id={"sp": me, "dp": my_x * 2 + 1 - my_core},
+            device_id_type=MESH,
+        )
+
+    own_parts = list(range(share))
+    extra_parts = list(range(2 * share - EXTRA, 2 * share)) if ny > 1 else []
+    other_parts = [i for i in range(share, PIECES) if i not in extra_parts]
+    sent_parts = own_parts + extra_parts
+    turns = own_parts[:-1] + other_parts[:1] + own_parts[-1:] + other_parts[1:] + extra_parts
+
+    def onward(i, yo):
+        return i < share and (i < share - EXTRA or yo < ny - 1)
+
+    def pass_on(turn):
+        j = turns[turn]
+        p = (first_piece + j) % PIECES
+        for o in range(1, chips):
+            wx_copy(o, p).wait_recv()
+            wc_copy(o, p).start()
+            for yo in range(1, ny):
+                if onward(j, yo):
+                    wy_copy(o, p, yo).start()
+
     param_copy(my_half).start()
+    for o in range(1, half):
+        for j in range(2):
+            qkv_copy(o, j).start()
+    loads[8].wait()
+    for j in sent_parts:
+        for o in range(1, chips):
+            wx_copy(o, (first_piece + j) % PIECES).start()
+    own_copy().start()
+    own_w = pltpu.make_async_copy(w_ref, wfull.at[my_dp], wl_sem)
+    own_w.start()
+    for j in range(2):
+        recv[j, my_rank] = send[my_rank + j * half]
+    for i in (7, 9, 10, 11, 12, 13, 14):
+        loads[i].wait()
 
     rows_in = plane * cap
     ids = index_ref[0].astype(jnp.float32)
@@ -284,7 +293,7 @@
     for o in range(1, nz):
         meta_copy((my_z + o) % nz, my_z).start()
 
-    stops = [PIECES * i // 8 for i in (2, 3, 4, 8, 8)]
+    stops = [PIECES * i // 8 for i in (2, 2, 4, 6, 8)]
 
     def pass_until(i):
         for j in range(stops[i - 1] if i else 0, stops[i]):
@@ -444,10 +453,14 @@
             for j in range(2):
                 mixed_copy(k + 1, j, my_rank).start()
 
+        @pl.when(k == half - 2)
+        def _():
+            pass_until(3)
+
         return 0
 
     lax.fori_loop(0, half, segment, 0)
-    pass_until(3)
+    pass_until(4)
     for j in range(2):
         mrecv[my_rank + j * half] = mixed[j, my_rank]
     sub_r = lax.broadcasted_iota(jnp.int32, (rows_in, tok), 0).astype(jnp.float32)
@@ -469,7 +482,6 @@
         all_of(meta.at[pl.ds(0, nz - 1)], meta_send, meta_recv).wait_recv()
     lax.fori_loop(0, nz, tables, 0)
     sig = jax.nn.sigmoid(logits_ref[0].astype(jnp.float32))
-    pass_until(4)
     if half > 1:
         mixed_all().wait_recv()
     gated = jnp.concatenate([mrecv[h].astype(jnp.float32) for h in range(n)], axis=1) * sig
@@ -507,29 +519,48 @@
     has_above, has_below = my_z + 1 < nz, my_z > 0
     edge = (my_z == 0) | (my_z == nz - 1)
 
-    def spread(z, p):
-        @pl.when((z <= my_z) & has_above)
+    inner_above = ~edge & (2 * my_z < nz - 1)
+    inner_below = ~edge & (2 * my_z >= nz - 1)
+
+    def spread(z, p, held=False):
+        @pl.when((z <= my_z) & has_above & ~(inner_above & held))
         def _():
             line_copy(z, p, above, up_send).start()
 
-        @pl.when((z >= my_z) & has_below)
+        @pl.when((z >= my_z) & has_below & ~(inner_below & held))
         def _():
             line_copy(z, p, below, down_send).start()
+
+    def release(p):
+        @pl.when(inner_above)
+        def _():
+            line_copy(my_z, p, above, up_send).start()
+
+        @pl.when(inner_below)
+        def _():
+            line_copy(my_z, p, below, down_send).start()
 
     for p in range(PARTS):
         line[my_z, p] = moe[:, p * part : (p + 1) * part]
-        spread(my_z, p)
+        spread(my_z, p, nz == 4 and p >= PARTS // 2)
     for p in range(PARTS):
         total[p] = s[:, p * part : (p + 1) * part]
     for i in (15, 16, 17):
         loads[i].wait()
     ff = hs.shape[1]
 
+    crossed = nz == 4
+
+    def order_of(z):
+        if crossed:
+            return ((0, 1, 3, 2), (1, 0, 3, 2), (2, 3, 0, 1), (3, 2, 0, 1))[z]
+        inner = 1 if 2 * z < nz - 1 else -1
+        return sorted(range(nz), key=lambda s: (abs(s - z), -(s - z) * inner))
+
     def by_distance(k):
         found = my_z
         for z in range(nz):
-            inner = 1 if 2 * z < nz - 1 else -1
-            near = sorted(range(nz), key=lambda s: (abs(s - z), -(s - z) * inner))
+            near = order_of(z)
             for place in range(nz):
                 found = jnp.where((my_z == z) & (k == place), near[place], found)
         return found
@@ -712,8 +743,18 @@
         def _():
             send_back(1)
 
+        if crossed:
+            @pl.when(~edge & last)
+            def _():
+                send_back(2)
+
         expert(k, edge & (k > 0))
         dispatch(k + 1, early, stop)
+        if crossed:
+            @pl.when(k == 0)
+            def _():
+                for p in range(midway, PARTS):
+                    release(p)
 
         @pl.when(edge & (k > 0))
         def _():
@@ -729,23 +770,26 @@
 
     @pl.when(~edge)
     def _():
-        for k in range(nz - 1, 1, -1):
+        for k in range(nz - 1, 2 if crossed else 1, -1):
             send_back(k)
         send_back(0)
-        if nz > 2:
+        if nz > 2 and not crossed:
             combine_all(1)
+        chained = (2, 1) if crossed else tuple(range(nz - 1, 1, -1))
 
         def one(s, _):
-            for behind in range(nz - 2):
+            for behind, k in enumerate(chained):
                 p = s - behind
 
                 @pl.when((p >= 0) & (p < PARTS))
                 def _():
-                    combine(by_distance(nz - 1 - behind), p)
+                    combine(by_distance(k), p)
 
             return 0
 
-        lax.fori_loop(0, PARTS + max(nz - 3, 0), one, 0)
+        lax.fori_loop(0, PARTS + max(len(chained) - 1, 0), one, 0)
+        if crossed:
+            combine_all(3)
 
     combine_all(0)
     for f in range(PARTS * SUBS):
@@ -789,7 +833,7 @@
     for o in range(chips):
         all_of(w_ref, wc_send.at[o], wc_recv.at[o]).wait_send()
     for o in range(1, chips):
-        held = w_ref.at[pl.ds(0, direct * piece)]
+        held = w_ref.at[pl.ds(0, len(sent_parts) * piece)]
         all_of(held, wx_send.at[o - 1], wc_recv.at[0]).wait_send()
         for yo in range(1, ny):
             held = w_ref.at[pl.ds(0, sum(onward(j, yo) for j in range(share)) * piece)]

time: 101 us -> 98.5 us (0.975)
  the two profiles are of different devices: /device:TPU:0 before, /device:TPU:8 now
where the time goes in v5:
time: 98.5 us; the launch traced here: 98.3 us
  Pallas kernels  97.5 us (99%)
    pallas_call x1, Pallas kernels, on_device(): pl.pallas_call(partial(layer_kernel, n=n, dpn=dpn, inputs=len(operands)),...  97.5 us

profile of v5, /device:TPU:8, one launch (start us, length us, event | category | flops | bytes accessed | tf_op | source)
XLA Modules:
  0.0 98.3 jit_solution(7148027286732956644)
XLA Ops:
  0.0 97.5 %shard_map.172 = bf16[1,128,2048]{2,1,0:T(8,128)(2,1)S(1)} custom-call(bf16[1,128,512]{2,1,0:T(8,128)(2,1)} %refs_0_.1, bf16[1,128,512]{2,1,0:T(8,128)(2,1)} %refs_1_.1, bf16[1,128,1024]{2,1,0:T(8,128)(2,1)} %refs_2_.1, bf16[1,32,128]{2,1,0:T(8,128)(2,1)} %bitcast.7, f32[1,2]{1,0:T(1,128)} %refs_4_.1, f32[1,1,1024]{2,1,0:T(1,128)} %refs_5_.1, ...), custom_call_target="tpu_custom_call" | custom-call | tf_op jit(solution)/shard_map/pallas_call | solution.py:883
  97.5 0.8 copy.20

commit v6 on v5

--- a/solution.py
+++ b/solution.py
@@ -12,9 +12,9 @@
 GATE_ROWS = 16
 PARTS = 4
 SUBS = 2
-FF_TILE = 256
+FF_TILE = 1024
 PIECES = 8
-EXTRA = 1
+EXTRA = 2
 
 
 def log_sigmoid(x):
@@ -736,7 +736,7 @@
     def tick(k, _):
         last = k == nz - 1
         stop = jnp.where(last, 0, PARTS)
-        early = jnp.minimum(jnp.where(k == 0, midway, jnp.where(edge, jnp.where(k == 1, midway // 2, midway), PARTS)), stop)
+        early = jnp.minimum(jnp.where(k == 0, midway, jnp.where(edge, jnp.where(k == 1, 0, 1), PARTS)), stop)
         dispatch(k + 1, 0, early)
 
         @pl.when(~edge & (k == nz - 2))

time: 98.5 us -> 94 us (0.954)
  Pallas kernels: 97.5 us -> 93.1 us
    pallas_call x1, Pallas kernels: 97.5 us -> 93.1 us  [on_device(): pl.pallas_call(partial(layer_kernel, n=n, dpn=dpn, inputs=len(operands)),...]
where the time goes in v6:
time: 94 us; the launch traced here: 93.9 us
  Pallas kernels  93.1 us (99%)
    pallas_call x1, Pallas kernels, on_device(): pl.pallas_call(partial(layer_kernel, n=n, dpn=dpn, inputs=len(operands)),...  93.1 us

profile of v6, /device:TPU:8, one launch (start us, length us, event | category | flops | bytes accessed | tf_op | source)
XLA Modules:
  0.0 93.9 jit_solution(12129441295272427237)
XLA Ops:
  0.0 93.1 %shard_map.172 = bf16[1,128,2048]{2,1,0:T(8,128)(2,1)S(1)} custom-call(bf16[1,128,512]{2,1,0:T(8,128)(2,1)} %refs_0_.1, bf16[1,128,512]{2,1,0:T(8,128)(2,1)} %refs_1_.1, bf16[1,128,1024]{2,1,0:T(8,128)(2,1)} %refs_2_.1, bf16[1,32,128]{2,1,0:T(8,128)(2,1)} %bitcast.7, f32[1,2]{1,0:T(1,128)} %refs_4_.1, f32[1,1,1024]{2,1,0:T(1,128)} %refs_5_.1, ...), custom_call_target="tpu_custom_call" | custom-call | tf_op jit(solution)/shard_map/pallas_call | solution.py:883
  93.1 0.8 copy.20
